TPU v7x, 32 devices: a whole 2x2x4 slice. The times are simulated.
32 devices in a mesh: sp: 16 (over z, y, x), tp: 2 (over core).
Axes of the slice: x: 2, y: 2, z: 4, core: 2. Of those that a mesh axis runs over, the one named last changes fastest.
Arguments:
- queries: bfloat16 [2048, 1024], P('sp', 'tp'), may hold values from -6 to 6
- keys: bfloat16 [2048, 1024], P('sp', 'tp'), may hold values from -6 to 6
- values: bfloat16 [2048, 2048], P('sp', 'tp'), may hold values from -6 to 6
- out_gate: bfloat16 [2048, 2048], P('sp', 'tp'), may hold values from -6 to 6
- decay_rate: float32 [8], P('tp'), may hold values from 0 to 1
- residual: bfloat16 [2048, 2048], P(('sp', 'tp')), may hold values from -6 to 6
- out_weight: bfloat16 [2048, 2048], P('tp'), may hold values from -0.125 to 0.125
- ffn_gain: float32 [2048], replicated, may hold values from 0.1 to 1.9
- route_ids: int32 [2048, 4], P(('sp', 'tp')), may hold values from 0 to 15, all different within a row; in each aligned block of 64 rows (0 to 63, 64 to 127, ...) at most 32 rows name the same one
- route_weights: float32 [2048, 4], P(('sp', 'tp')), may hold values from 0.1 to 1
- gate_up: bfloat16 [16, 2048, 2048], P('sp', None, 'tp'), may hold values from -0.375 to 0.375
- lin_up: bfloat16 [16, 2048, 2048], P('sp', None, 'tp'), may hold values from -0.375 to 0.375
- down_weight: bfloat16 [16, 2048, 2048], P('sp', 'tp'), may hold values from -0.03125 to 0.03125
Outputs:
- layer_out: bfloat16 [2048, 2048], P(('sp', 'tp'))
Inputs may be any that keep to these rules, and one draw needn't show every extreme that they name: `route_ids`: within the rows of one device (aligned blocks of 64 rows), no expert is named by more than 32 entries, a bound that some block reaches; the 4 experts of a row differ.
All inputs are finite; a program needn't handle non-finite values.
Results may differ from a plain program's by a relative error of at most 0.03.
Values may be sent and summed in bfloat16 or wider, within the bound.
No kernel may reach another device: no remote copies, remote signals or barrier semaphores. Data moves between devices by JAX's collectives and lax.ppermute only.
A program may use at most 128 MiB of HBM per device.

v0:
```python
import functools

import jax
import jax.numpy as jnp
from jax import lax
from jax.experimental import pallas as pl
from jax.experimental.pallas import tpu as pltpu
from jax.sharding import PartitionSpec as P


DK = 128
DV = 256
EPS = 1e-05
CLAMP_LIMIT = 7.0
SIGMOID_SLOPE = 1.702
HIDDEN = 512


class Spec:
    def __init__(self, seen, lies=None):
        self.block, self.lies = pl.BlockSpec(memory_space=seen), lies

    def place(self, arg):
        return arg if self.lies is None else pltpu.with_memory_space_constraint(arg, self.lies)


SCALAR = Spec(pltpu.SMEM)
SMEM = Spec(pltpu.SMEM, pltpu.HBM)
VMEM = Spec(pltpu.VMEM, pltpu.HBM)
NEAR = Spec(pltpu.VMEM, pltpu.VMEM)
FAR = Spec(pl.ANY, pltpu.HBM)
AFTER = Spec(pl.ANY)


def head_cols(h, width):
    return slice(h * width, (h + 1) * width)


def head_state(keys_ref, values_ref, head, rate):
    block_len = keys_ref.shape[0]
    left = block_len - 1.0 - lax.broadcasted_iota(jnp.int32, (block_len, DK), 0).astype(jnp.float32)
    k = keys_ref[:, pl.ds(pl.multiple_of(head * DK, DK), DK)].astype(jnp.float32)
    k = (k * jnp.exp(left * -rate) * DK ** (-0.5)).astype(jnp.bfloat16)
    return lax.dot_general(
        k,
        values_ref[:, pl.ds(pl.multiple_of(head * DV, DV), DV)],
        (((0,), (0,)), ((), ())),
        preferred_element_type=jnp.float32,
    ).astype(jnp.bfloat16)


def state_kernel(me_ref, decay_ref, keys_ref, values_ref, *outs):
    for near, out_ref in enumerate(outs):
        head = jnp.bitwise_xor(jnp.bitwise_and(me_ref[0], len(outs) - 1), near)
        out_ref[...] = head_state(keys_ref, values_ref, head, decay_ref[head])


def decayed(part, rate, blocks):
    return part.astype(jnp.float32) * jnp.exp(jnp.full((1, part.shape[1]), -rate * blocks))


def total_kernel(block_len, me_ref, decay_ref, ids_ref, weights_ref, *refs):
    parts, out_ref = refs[:-1], refs[-1]
    inner = len(parts)
    plane = jnp.bitwise_and(me_ref[0], inner - 1)
    rate = decay_ref[plane] * block_len
    total = 0.0
    for near, part in enumerate(parts):
        later = inner - 1 - jnp.bitwise_xor(plane, near)
        total = total + decayed(part[...], rate, later.astype(jnp.float32))
    top, rows = ids_ref.shape
    weight = weights_ref[...]
    high = weight.astype(jnp.bfloat16).astype(jnp.float32)
    tile = jnp.concatenate(
        [
            jnp.concatenate([ids_ref[...].astype(jnp.float32), high], axis=0),
            jnp.concatenate([jnp.zeros((top, rows), jnp.float32), weight - high], axis=0),
            jnp.zeros((2 * top, DV - 2 * rows), jnp.float32),
        ],
        axis=1,
    )
    out_ref[:DK, :] = total.astype(jnp.bfloat16)
    out_ref[DK:, :] = tile.astype(jnp.bfloat16)


def prefix_kernel(block_len, blocks, inner, me_ref, decay_ref, *refs):
    parts, totals = refs[:inner], refs[inner : inner + len(blocks)]
    outs, info_ref = refs[inner + len(blocks) : -1], refs[-1]
    me = me_ref[0]
    plane = jnp.bitwise_and(me, inner - 1)
    layer = lax.div(me, inner)
    rate = decay_ref[plane] * block_len
    before = jnp.zeros((DK, DV), jnp.float32)
    for n, distance in enumerate(blocks):
        info_ref[n] = totals[n][DK:, :].astype(jnp.float32)
        if distance:
            term = decayed(totals[n][:DK, :], rate, inner * (distance - 1.0))
            before = before + jnp.where(layer >= distance, term, 0.0)
    for near, out_ref in enumerate(outs):
        target = jnp.bitwise_xor(plane, near)
        total = decayed(before, rate, target.astype(jnp.float32))
        for other, part in enumerate(parts):
            source = jnp.bitwise_xor(plane, other)
            later = jnp.maximum(target - 1 - source, 0).astype(jnp.float32)
            total = total + jnp.where(source < target, decayed(part[...], rate, later), 0.0)
        out_ref[...] = total.astype(jnp.bfloat16)


def intra_kernel(decay_ref, q_ref, k_ref, v_ref, gate_ref, intra_ref, silu_ref):
    block_len = q_ref.shape[0]
    ahead = lax.broadcasted_iota(jnp.int32, (block_len, block_len), 0) - lax.broadcasted_iota(
        jnp.int32, (block_len, block_len), 1
    )
    causal = ahead >= 0
    ahead = jnp.where(causal, ahead, 0).astype(jnp.float32)
    for h in range(decay_ref.shape[0]):
        scores = lax.dot_general(
            q_ref[:, head_cols(h, DK)],
            k_ref[:, head_cols(h, DK)],
            (((1,), (1,)), ((), ())),
            preferred_element_type=jnp.float32,
        )
        scores = scores * jnp.where(causal, jnp.exp(ahead * -decay_ref[h]), 0.0) * DK ** (-0.5)
        intra_ref[:, head_cols(h, DV)] = jnp.dot(
            scores.astype(jnp.bfloat16),
            v_ref[:, head_cols(h, DV)],
            preferred_element_type=jnp.float32,
        )
    gate = gate_ref[...].astype(jnp.float32)
    silu_ref[...] = gate / (1.0 + jnp.exp(-gate))


def mix_kernel(
    me_ref,
    decay_ref,
    tp_ref,
    q_ref,
    intra_ref,
    silu_ref,
    weight_hbm,
    *refs,
):
    heads = decay_ref.shape[0]
    states, (keep_ref, send_ref, state_ref, weight_ref, sems) = refs[:heads], refs[heads:]
    plane = jnp.bitwise_and(me_ref[0], heads - 1)
    for near in range(heads):
        state_ref[near] = states[near][...]
    copies = [
        pltpu.make_async_copy(
            weight_hbm.at[head_cols(h, DV)], weight_ref.at[head_cols(h, DV)], sems.at[h]
        )
        for h in range(heads)
    ]
    for copy in copies:
        copy.start()
    block_len = q_ref.shape[0]
    lead = 1.0 + lax.broadcasted_iota(jnp.int32, (block_len, DV), 0).astype(jnp.float32)
    gated = []
    for h in range(heads):
        cross = jnp.dot(
            q_ref[:, head_cols(h, DK)],
            state_ref[jnp.bitwise_xor(plane, h)],
            preferred_element_type=jnp.float32,
        )
        retained = intra_ref[:, head_cols(h, DV)] + cross * jnp.exp(lead * -decay_ref[h])
        normed = retained * lax.rsqrt(jnp.mean(retained * retained, axis=-1, keepdims=True) + EPS)
        gated.append((normed * silu_ref[:, head_cols(h, DV)]).astype(jnp.bfloat16))
    total = jnp.zeros((block_len, weight_ref.shape[1]), jnp.float32)
    for h in range(heads):
        copies[h].wait()
        total = total + jnp.dot(
            gated[h], weight_ref[head_cols(h, DV), :], preferred_element_type=jnp.float32
        )
    total = total.astype(jnp.bfloat16)
    first, second = total[: block_len // 2], total[block_len // 2 :]
    mine = tp_ref[0] == 0

    @pl.when(mine)
    def _():
        keep_ref[...] = first
        send_ref[...] = second

    @pl.when(jnp.logical_not(mine))
    def _():
        keep_ref[...] = second
        send_ref[...] = first


def norm_kernel(residual_ref, keep_ref, got_ref, gain_ref, mixed_ref, rows_ref):
    mixed = (
        residual_ref[...].astype(jnp.float32)
        + keep_ref[...].astype(jnp.float32)
        + got_ref[...].astype(jnp.float32)
    ).astype(jnp.bfloat16)
    mixed_ref[...] = mixed
    wide = mixed.astype(jnp.float32)
    rows_ref[...] = (
        wide * lax.rsqrt(jnp.mean(wide * wide, axis=-1, keepdims=True) + EPS) * gain_ref[...]
    ).astype(jnp.bfloat16)


def slot_table(me, info, inner, capacity, rows, top):
    plane = jnp.bitwise_and(me, inner - 1)
    near = lax.broadcasted_iota(jnp.int32, (inner, rows), 0)
    expert = (me - plane + jnp.bitwise_xor(near, plane)).astype(jnp.float32)
    named = jnp.zeros((inner, rows), jnp.float32)
    weight = jnp.zeros((inner, rows), jnp.float32)
    for k in range(top):
        hit = info[k : k + 1, :rows] == expert
        named = named + jnp.where(hit, 1.0, 0.0)
        given = info[top + k : top + k + 1, :rows] + info[top + k : top + k + 1, rows : 2 * rows]
        weight = weight + jnp.where(hit, given, 0.0)
    before = lax.broadcasted_iota(jnp.int32, (rows, rows), 0) < lax.broadcasted_iota(
        jnp.int32, (rows, rows), 1
    )
    rank = jnp.dot(
        named.astype(jnp.bfloat16),
        jnp.where(before, 1.0, 0.0).astype(jnp.bfloat16),
        preferred_element_type=jnp.float32,
    )
    rank = jnp.where(named > 0.0, rank, -1.0).astype(jnp.int32)
    slot = lax.broadcasted_iota(jnp.int32, (inner, capacity, rows), 1)
    return jnp.where(rank[:, None, :] == slot, 1.0, 0.0), weight


def halves_kernel(low_ref, high_ref, *refs):
    first_ref, second_ref = refs[-2:]
    half = first_ref.shape[0]
    first_ref[...] = low_ref[:half, :]
    second_ref[...] = high_ref[half:, :]


def gather_kernel(places, capacity, top, inner, counts, me_ref, info_ref, *refs):
    outs = refs[len(refs) - inner :]
    at = 0
    for n, place in enumerate(places):
        source = jnp.concatenate([ref[...] for ref in refs[at : at + counts[n]]], axis=0)
        at += counts[n]
        rows = source.shape[0]
        table, _ = slot_table(me_ref[0], info_ref[place], inner, capacity, rows, top)
        table = table.reshape(inner * capacity, rows).astype(jnp.bfloat16)
        slots = jnp.dot(table, source, preferred_element_type=jnp.float32).astype(jnp.bfloat16)
        for r in range(inner):
            outs[r][n * capacity : (n + 1) * capacity, :] = slots[r * capacity : (r + 1) * capacity]


def combine_kernel(places, capacity, top, inner, me_ref, info_ref, *refs):
    parts, outs = refs[:inner], refs[inner : inner + len(places)]
    for n, place in enumerate(places):
        rows = outs[n].shape[0]
        table, weight = slot_table(me_ref[0], info_ref[place], inner, capacity, rows, top)
        table = (table * weight[:, None, :]).reshape(inner * capacity, rows)
        high = table.astype(jnp.bfloat16)
        low = (table - high.astype(jnp.float32)).astype(jnp.bfloat16)
        slots = jnp.concatenate(
            [part[n * capacity : (n + 1) * capacity, :] for part in parts], axis=0
        )
        turned = (((0,), (0,)), ((), ()))
        total = lax.dot_general(high, slots, turned, preferred_element_type=jnp.float32)
        total = total + lax.dot_general(low, slots, turned, preferred_element_type=jnp.float32)
        outs[n][...] = total.astype(outs[n].dtype)


def final_kernel(mixed_ref, *refs):
    total = mixed_ref[...].astype(jnp.float32)
    for ref in refs[:-1]:
        total = total + ref[...].astype(jnp.float32)
    refs[-1][...] = total.astype(jnp.bfloat16)


def call(kernel, out_shape, specs, flops=1 << 28, mib=8, in_vmem=True, scratch=()):
    single = not isinstance(out_shape, (tuple, list))
    shapes = (out_shape,) if single else tuple(out_shape)
    if in_vmem:
        shapes = tuple(pltpu.VMEM(part.shape, part.dtype) for part in shapes)
    whole = pl.BlockSpec(memory_space=pltpu.VMEM)
    run = pl.pallas_call(
        kernel,
        out_shape=shapes[0] if single else shapes,
        in_specs=[spec.block for spec in specs],
        out_specs=whole if single else tuple(whole for _ in shapes),
        scratch_shapes=scratch,
        compiler_params=pltpu.CompilerParams(vmem_limit_bytes=mib << 20),
        cost_estimate=pl.CostEstimate(flops=flops, bytes_accessed=1 << 20, transcendentals=0),
    )

    def placed(*args):
        return run(*(spec.place(arg) for spec, arg in zip(specs, args, strict=True)))

    return placed


def bf16(*shape):
    return jax.ShapeDtypeStruct(shape, jnp.bfloat16)


def expert_kernel(parts, gives, *refs):
    sources, weights, refs = refs[:parts], refs[parts : parts + 6], refs[parts + 6 :]
    gate, lin, down, total, sems = refs[len(refs) - 5 :]
    outs = refs[len(refs) - 5 - gives : len(refs) - 5]
    slots, _, hidden = gate.shape
    half = weights[0].shape[1] // hidden

    def copies(at, source):
        slot = lax.rem(at, slots)
        block = pl.ds(pl.multiple_of(lax.rem(at, half) * hidden, hidden), hidden)
        gate_hbm, lin_hbm, down_hbm = source
        return (
            pltpu.make_async_copy(gate_hbm.at[:, block], gate.at[slot], sems.at[0, slot]),
            pltpu.make_async_copy(lin_hbm.at[:, block], lin.at[slot], sems.at[1, slot]),
            pltpu.make_async_copy(down_hbm.at[block, :], down.at[slot], sems.at[2, slot]),
        )

    def start(at):
        @pl.when(at < half)
        def _():
            for copy in copies(at, weights[:3]):
                copy.start()

        @pl.when(jnp.logical_and(at >= half, at < 2 * half))
        def _():
            for copy in copies(at, weights[3:]):
                copy.start()

    for at in range(slots - 1):
        start(jnp.int32(at))
    rows = jnp.concatenate([source[...] for source in sources], axis=0)
    total[...] = jnp.zeros_like(total)

    def step(at, _):
        start(at + slots - 1)
        slot = lax.rem(at, slots)
        arrive = copies(at, weights[:3])
        arrive[0].wait()
        pre = jnp.dot(rows, gate[slot], preferred_element_type=jnp.float32)
        clipped = jnp.minimum(pre, CLAMP_LIMIT)
        act = clipped / (1.0 + jnp.exp(-SIGMOID_SLOPE * clipped))
        arrive[1].wait()
        pre = jnp.dot(rows, lin[slot], preferred_element_type=jnp.float32)
        act = (act * (jnp.clip(pre, -CLAMP_LIMIT, CLAMP_LIMIT) + 1.0)).astype(jnp.bfloat16)
        arrive[2].wait()
        total[...] += jnp.dot(act, down[slot], preferred_element_type=jnp.float32)
        return 0

    lax.fori_loop(0, 2 * half, step, 0)
    at = 0
    for out_ref in outs:
        each = out_ref.shape[0]
        out_ref[...] = total[at : at + each, :].astype(jnp.bfloat16)
        at += each


def run_experts(sources, gives, own, other, after, hidden=HIDDEN, slots=2):
    count, width = sum(source.shape[0] for source in sources), sources[0].shape[1]
    run = call(
        functools.partial(expert_kernel, len(sources), gives),
        tuple(bf16(count // gives, width) for _ in range(gives)),
        [NEAR] * len(sources) + [FAR] * 6 + [AFTER] * len(after),
        flops=12 * count * width * own[0].shape[1],
        mib=40,
        scratch=[
            pltpu.VMEM((slots, width, hidden), jnp.bfloat16),
            pltpu.VMEM((slots, width, hidden), jnp.bfloat16),
            pltpu.VMEM((slots, hidden, width), jnp.bfloat16),
            pltpu.VMEM((count, width), jnp.float32),
            pltpu.SemaphoreType.DMA((3, slots)),
        ],
    )
    return run(*sources, *own, *other, *after)


def local(
    queries,
    keys,
    values,
    out_gate,
    decay_rate,
    residual,
    out_weight,
    ffn_gain,
    route_ids,
    route_weights,
    gate_up,
    lin_up,
    down_weight,
):
    sp, tp = lax.axis_size("sp"), lax.axis_size("tp")
    block_len = queries.shape[0]
    heads = decay_rate.shape[0]
    width = residual.shape[1]
    own_rows, top = route_ids.shape
    swap = [(i, (i + 1) % tp) for i in range(tp)]
    mine = (gate_up[0], lin_up[0], down_weight[0])
    other = [lax.ppermute(part, "tp", swap) for part in mine]
    me = lax.axis_index("sp").reshape(1)

    inner = heads
    outer = sp // inner
    blocks = sorted(range(outer), key=lambda d: (min(d, outer - d), -d))
    capacity = own_rows * top * tp // sp

    def to_plane(part, distance):
        return lax.ppermute(part, "sp", [(i, (i + distance * inner) % sp) for i in range(sp)])

    def in_plane(part, near):
        return lax.ppermute(part, "sp", [(i, i ^ near) for i in range(sp)])

    near_chips = range(1, inner)
    sums = call(state_kernel, (bf16(DK, DV),) * inner, [SCALAR, SMEM, VMEM, VMEM])(
        me, decay_rate, keys, values
    )
    sums = [sums[0]] + [in_plane(sums[r], r) for r in near_chips]
    total = call(
        functools.partial(total_kernel, block_len),
        bf16(DK + 2 * top, DV),
        [SCALAR, SMEM, VMEM, VMEM] + [NEAR] * inner,
    )(me, decay_rate, route_ids.T, route_weights.T, *sums)
    *carried, info = call(
        functools.partial(prefix_kernel, block_len, blocks, inner),
        (bf16(DK, DV),) * inner + (jax.ShapeDtypeStruct((outer, 2 * top, DV), jnp.float32),),
        [SCALAR, SMEM] + [NEAR] * (inner + outer),
    )(me, decay_rate, *sums, *(to_plane(total, d) if d else total for d in blocks))
    carried = [carried[0]] + [in_plane(carried[r], r) for r in near_chips]

    term = jax.ShapeDtypeStruct((block_len, heads * DV), jnp.float32)
    intra, silu = call(intra_kernel, (term, term), [SMEM] + [VMEM] * 4, flops=1 << 32)(
        decay_rate, queries, keys, values, out_gate
    )
    keep, send = call(
        mix_kernel,
        (bf16(own_rows, width), bf16(own_rows, width)),
        [SCALAR, SMEM, SCALAR, VMEM, NEAR, NEAR, FAR] + [NEAR] * inner,
        mib=16,
        scratch=[
            pltpu.VMEM((heads, DK, DV), jnp.bfloat16),
            pltpu.VMEM(out_weight.shape, jnp.bfloat16),
            pltpu.SemaphoreType.DMA((heads,)),
        ],
    )(me, decay_rate, lax.axis_index("tp").reshape(1), queries, intra, silu, out_weight, *carried)
    got = lax.ppermute(send, "tp", swap)
    mixed, rows = call(
        norm_kernel, (bf16(own_rows, width), bf16(own_rows, width)), [VMEM, NEAR, NEAR, VMEM]
    )(residual, keep, got, ffn_gain.reshape(1, width))

    size = max(1, outer // 4)
    groups = [range(i, min(i + size, outer)) for i in range(0, outer, size)]
    across = outer // 2 if outer > 2 and outer % 2 == 0 and size == 1 else None
    at = {d: (to_plane(rows, d) if d else rows,) for d in blocks if d != across}

    def send_slots(places, after):
        parts = [part for n in places for part in at[blocks[n]]]
        slots = call(
            functools.partial(
                gather_kernel, places, capacity, top, inner, [len(at[blocks[n]]) for n in places]
            ),
            tuple(bf16(len(places) * capacity, width) for _ in range(inner)),
            [SCALAR] + [NEAR] * (1 + len(parts)) + [AFTER] * len(after),
        )(me, info, *parts, *after)
        return [slots[0]] + [in_plane(slots[r], r) for r in near_chips], [slots[0]]

    sent, after = [], []
    for g, places in enumerate(groups):
        if g == 1 and across:
            pair = call(
                halves_kernel, (bf16(own_rows // 2, width),) * 2, [NEAR] * 2 + [AFTER] * len(after)
            )(at[across - 1][0], at[across + 1][0], *after)
            at[across] = (to_plane(pair[0], 1), to_plane(pair[1], -1))
            after = [pair[0]]
        slots, after = send_slots(places, after)
        sent.append(slots)

    def send_home(places, parts):
        parts = [parts[0]] + [in_plane(parts[r], r) for r in near_chips]
        kinds = [jnp.bfloat16 if blocks[n] else jnp.float32 for n in places]
        sums = call(
            functools.partial(combine_kernel, places, capacity, top, inner),
            tuple(jax.ShapeDtypeStruct((own_rows, width), kind) for kind in kinds),
            [SCALAR] + [NEAR] * (1 + inner),
        )(me, info, *parts)
        return [
            to_plane(part, -blocks[n]) if blocks[n] else part
            for n, part in zip(places, sums, strict=True)
        ]

    half = (len(groups) + 1) // 2
    first = [slots[r] for r in range(inner) for slots in sent[:half]]
    early = run_experts(first, inner, mine, other, after)
    second = [slots[r] for slots in reversed(sent[half:]) for r in range(inner)]
    late = run_experts(second, len(second), mine, other, early[:1])
    home = send_home([n for places in groups[:half] for n in places], early)
    for g, places in enumerate(reversed(groups[half:])):
        home += send_home(places, late[g * inner : (g + 1) * inner])
    return call(final_kernel, bf16(own_rows, width), [NEAR] * (1 + len(home)), in_vmem=False)(
        mixed, *home
    )


def solution(mesh):
    placed = (
        P("sp", "tp"),
        P("sp", "tp"),
        P("sp", "tp"),
        P("sp", "tp"),
        P("tp"),
        P(("sp", "tp"), None),
        P("tp", None),
        P(),
        P(("sp", "tp"), None),
        P(("sp", "tp"), None),
        P("sp", None, "tp"),
        P("sp", None, "tp"),
        P("sp", "tp", None),
    )
    return jax.shard_map(
        local, mesh=mesh, in_specs=placed, out_specs=P(("sp", "tp"), None), check_vma=False
    )
```

profile of v0, /device:TPU:0, one launch (start us, length us, event | category | flops | bytes accessed | tf_op | source)
XLA Modules:
  0.0 147.9 jit_solution(9238313037626142457)
XLA Ops:
  2.3 2.5 %collective-permute-start = (bf16[128,256]{1,0:T(8,128)(2,1)S(1)}, bf16[128,256]{1,0:T(8,128)(2,1)S(1)}, u32[]{:S(2)}, u32[]{:S(2)}) collective-permute-start(bf16[128,256]{1,0:T(8,128)(2,1)S(1)} %get-tuple-element.55), channel_id=1, source_target_pairs={{0,2},{2,0},{4,6},{6,4},{8,10},{10,8},{12,14},{14,12},{16,18},{18,... | collective-permute-start | bytes 196616 | tf_op jit(solution)/shard_map/ppermute | solution.py:406
  7.6 2.7 %collective-permute-start.2 = (bf16[128,256]{1,0:T(8,128)(2,1)S(1)}, bf16[128,256]{1,0:T(8,128)(2,1)S(1)}, u32[]{:S(2)}, u32[]{:S(2)}) collective-permute-start(bf16[128,256]{1,0:T(8,128)(2,1)S(1)} %get-tuple-element.57), channel_id=1, source_target_pairs={{0,6},{2,4},{4,2},{6,0},{8,14},{10,12},{12,10},{14,8},{16,22},{18,... | collective-permute-start | bytes 196616 | tf_op jit(solution)/shard_map/ppermute | solution.py:406
  10.3 2.5 %collective-permute-done.2.refs_3_ = bf16[128,256]{1,0:T(8,128)(2,1)S(1)} collective-permute-done((bf16[128,256]{1,0:T(8,128)(2,1)S(1)}, bf16[128,256]{1,0:T(8,128)(2,1)S(1)}, u32[]{:S(2)}, u32[]{:S(2)}) %collective-permute-start.2) | collective-permute-done | bytes 65568 | tf_op jit(solution)/shard_map/ppermute | solution.py:406
  13.6 2.8 %collective-permute-start.5 = (bf16[136,256]{1,0:T(8,128)(2,1)S(1)}, bf16[136,256]{1,0:T(8,128)(2,1)S(1)}, u32[]{:S(2)}, u32[]{:S(2)}) collective-permute-start(bf16[136,256]{1,0:T(8,128)(2,1)S(1)} %shard_map.129.refs_4_), channel_id=1, source_target_pairs={{0,16},{2,18},{4,20},{6,22},{8,24},{10,26},{12,28},{14,30},{16,0},... | collective-permute-start | bytes 208904 | tf_op jit(solution)/shard_map/ppermute | solution.py:403
  18.9 4.5 %collective-permute-start.3 = (bf16[136,256]{1,0:T(8,128)(2,1)S(1)}, bf16[136,256]{1,0:T(8,128)(2,1)S(1)}, u32[]{:S(2)}, u32[]{:S(2)}) collective-permute-start(bf16[136,256]{1,0:T(8,128)(2,1)S(1)} %shard_map.129.refs_4_), channel_id=1, source_target_pairs={{0,24},{2,26},{4,28},{6,30},{8,0},{10,2},{12,4},{14,6},{16,8},{18,... | collective-permute-start | bytes 208904 | tf_op jit(solution)/shard_map/ppermute | solution.py:403
  30.9 2.1 %collective-permute-start.8 = (bf16[128,256]{1,0:T(8,128)(2,1)S(1)}, bf16[128,256]{1,0:T(8,128)(2,1)S(1)}, u32[]{:S(2)}, u32[]{:S(2)}) collective-permute-start(bf16[128,256]{1,0:T(8,128)(2,1)S(1)} %get-tuple-element.61), channel_id=1, source_target_pairs={{0,6},{2,4},{4,2},{6,0},{8,14},{10,12},{12,10},{14,8},{16,22},{18,... | collective-permute-start | bytes 196616 | tf_op jit(solution)/shard_map/ppermute | solution.py:406
  36.0 3.5 %shard_map.131 = (bf16[64,2048]{1,0:T(8,128)(2,1)S(1)}, bf16[64,2048]{1,0:T(8,128)(2,1)S(1)}) custom-call(s32[1]{0:T(128)} %bitcast.me_ref, f32[4]{0:T(128)} %decay_ref.9, s32[1]{0:T(128)} %bitcast.1.tp_ref, bf16[128,512]{1,0:T(8,128)(2,1)} %q_ref.3, f32[128,1024]{1,0:T(8,128)S(1)} %get-tuple-element.52.intra_ref, ...), custom_call_target="tpu_custom_call" | custom-call | flops 268435456 | bytes 1048576 | tf_op jit(solution)/shard_map/pallas_call | solution.py:288
  44.6 3.8 %collective-permute-done.12.refs_2_ = bf16[32,2048]{1,0:T(8,128)(2,1)S(1)} collective-permute-done((bf16[32,2048]{1,0:T(8,128)(2,1)S(1)}, bf16[32,2048]{1,0:T(8,128)(2,1)S(1)}, u32[]{:S(2)}, u32[]{:S(2)}) %collective-permute-start.12) | collective-permute-done | bytes 131104 | tf_op jit(solution)/shard_map/ppermute | solution.py:406
  48.4 3.9 %collective-permute-start.10 = (bf16[64,2048]{1,0:T(8,128)(2,1)S(1)}, bf16[64,2048]{1,0:T(8,128)(2,1)S(1)}, u32[]{:S(2)}, u32[]{:S(2)}) collective-permute-start(bf16[64,2048]{1,0:T(8,128)(2,1)S(1)} %get-tuple-element.66.refs_0_), channel_id=1, source_target_pairs={{0,24},{2,26},{4,28},{6,30},{8,0},{10,2},{12,4},{14,6},{16,8},{18,... | collective-permute-start | bytes 786440 | tf_op jit(solution)/shard_map/ppermute | solution.py:403
  52.3 3.2 %collective-permute-done.11.low_ref.refs_0_ = bf16[64,2048]{1,0:T(8,128)(2,1)S(1)} collective-permute-done((bf16[64,2048]{1,0:T(8,128)(2,1)S(1)}, bf16[64,2048]{1,0:T(8,128)(2,1)S(1)}, u32[]{:S(2)}, u32[]{:S(2)}) %collective-permute-start.11) | collective-permute-done | bytes 262176 | tf_op jit(solution)/shard_map/ppermute | solution.py:403
  56.9 3.3 %collective-permute-done.10.high_ref.refs_0_ = bf16[64,2048]{1,0:T(8,128)(2,1)S(1)} collective-permute-done((bf16[64,2048]{1,0:T(8,128)(2,1)S(1)}, bf16[64,2048]{1,0:T(8,128)(2,1)S(1)}, u32[]{:S(2)}, u32[]{:S(2)}) %collective-permute-start.10) | collective-permute-done | bytes 262176 | tf_op jit(solution)/shard_map/ppermute | solution.py:403
  61.7 5.2 %collective-permute-start.22 = (bf16[32,2048]{1,0:T(8,128)(2,1)S(1)}, bf16[32,2048]{1,0:T(8,128)(2,1)S(1)}, u32[]{:S(2)}, u32[]{:S(2)}) collective-permute-start(bf16[32,2048]{1,0:T(8,128)(2,1)S(1)} %get-tuple-element.76), channel_id=1, source_target_pairs={{0,24},{2,26},{4,28},{6,30},{8,0},{10,2},{12,4},{14,6},{16,8},{18,... | collective-permute-start | bytes 393224 | tf_op jit(solution)/shard_map/ppermute | solution.py:403
  69.4 4.9 %collective-permute-done.21.refs_0_ = bf16[32,2048]{1,0:T(8,128)(2,1)S(1)} collective-permute-done((bf16[32,2048]{1,0:T(8,128)(2,1)S(1)}, bf16[32,2048]{1,0:T(8,128)(2,1)S(1)}, u32[]{:S(2)}, u32[]{:S(2)}) %collective-permute-start.21) | collective-permute-done | bytes 131104 | tf_op jit(solution)/shard_map/ppermute | solution.py:403
  76.3 3.7 %collective-permute-done.15.refs_5_ = bf16[32,2048]{1,0:T(8,128)(2,1)S(1)} collective-permute-done((bf16[32,2048]{1,0:T(8,128)(2,1)S(1)}, bf16[32,2048]{1,0:T(8,128)(2,1)S(1)}, u32[]{:S(2)}, u32[]{:S(2)}) %collective-permute-start.15) | collective-permute-done | bytes 131104 | tf_op jit(solution)/shard_map/ppermute | solution.py:406
  82.8 3.6 %collective-permute-done.30.refs_5_ = bf16[32,2048]{1,0:T(8,128)(2,1)S(1)} collective-permute-done((bf16[32,2048]{1,0:T(8,128)(2,1)S(1)}, bf16[32,2048]{1,0:T(8,128)(2,1)S(1)}, u32[]{:S(2)}, u32[]{:S(2)}) %collective-permute-start.30) | collective-permute-done | bytes 131104 | tf_op jit(solution)/shard_map/ppermute | solution.py:406
  86.6 2.0 %collective-permute-start.27 = (bf16[32,2048]{1,0:T(8,128)(2,1)S(1)}, bf16[32,2048]{1,0:T(8,128)(2,1)S(1)}, u32[]{:S(2)}, u32[]{:S(2)}) collective-permute-start(bf16[32,2048]{1,0:T(8,128)(2,1)S(1)} %get-tuple-element.85), channel_id=1, source_target_pairs={{0,2},{2,0},{4,6},{6,4},{8,10},{10,8},{12,14},{14,12},{16,18},{18,... | collective-permute-start | bytes 393224 | tf_op jit(solution)/shard_map/ppermute | solution.py:406
  90.1 10.7 %shard_map.138 = (bf16[64,2048]{1,0:T(8,128)(2,1)S(1)}, bf16[64,2048]{1,0:T(8,128)(2,1)S(1)}, bf16[64,2048]{1,0:T(8,128)(2,1)S(1)}, bf16[64,2048]{1,0:T(8,128)(2,1)S(1)}) custom-call(bf16[32,2048]{1,0:T(8,128)(2,1)S(1)} %get-tuple-element.67.refs_0_, bf16[32,2048]{1,0:T(8,128)(2,1)S(1)} %get-tuple-element.69.refs_1_, ...), custom_call_target="tpu_custom_call" | custom-call | flops 6442450944 | bytes 1048576 | tf_op jit(solution)/shard_map/pallas_call | solution.py:288
  100.9 10.7 %shard_map.140 = (bf16[32,2048]{1,0:T(8,128)(2,1)S(1)}, bf16[32,2048]{1,0:T(8,128)(2,1)S(1)}, bf16[32,2048]{1,0:T(8,128)(2,1)S(1)}, bf16[32,2048]{1,0:T(8,128)(2...) custom-call(bf16[32,2048]{1,0:T(8,128)(2,1)S(1)} %get-tuple-element., ...), custom_call_target="tpu_custom_call" | custom-call | flops 6442450944 | bytes 1048576 | tf_op jit(solution)/shard_map/pallas_call | solution.py:288
  114.9 2.1 %collective-permute-start.39 = (bf16[32,2048]{1,0:T(8,128)(2,1)S(1)}, bf16[32,2048]{1,0:T(8,128)(2,1)S(1)}, u32[]{:S(2)}, u32[]{:S(2)}) collective-permute-start(bf16[32,2048]{1,0:T(8,128)(2,1)S(1)} %get-tuple-element.98), channel_id=1, source_target_pairs={{0,6},{2,4},{4,2},{6,0},{8,14},{10,12},{12,10},{14,8},{16,22},{18,... | collective-permute-start | bytes 393224 | tf_op jit(solution)/shard_map/ppermute | solution.py:406
  120.8 2.7 %collective-permute-start.25 = (bf16[64,2048]{1,0:T(8,128)(2,1)S(1)}, bf16[64,2048]{1,0:T(8,128)(2,1)S(1)}, u32[]{:S(2)}, u32[]{:S(2)}) collective-permute-start(bf16[64,2048]{1,0:T(8,128)(2,1)S(1)} %get-tuple-element.82), channel_id=1, source_target_pairs={{0,6},{2,4},{4,2},{6,0},{8,14},{10,12},{12,10},{14,8},{16,22},{18,... | collective-permute-start | bytes 786440 | tf_op jit(solution)/shard_map/ppermute | solution.py:406
  124.2 2.1 %collective-permute-start.35 = (bf16[32,2048]{1,0:T(8,128)(2,1)S(1)}, bf16[32,2048]{1,0:T(8,128)(2,1)S(1)}, u32[]{:S(2)}, u32[]{:S(2)}) collective-permute-start(bf16[32,2048]{1,0:T(8,128)(2,1)S(1)} %get-tuple-element.94), channel_id=1, source_target_pairs={{0,6},{2,4},{4,2},{6,0},{8,14},{10,12},{12,10},{14,8},{16,22},{18,... | collective-permute-start | bytes 393224 | tf_op jit(solution)/shard_map/ppermute | solution.py:406
  126.8 5.5 %collective-permute-done.34.refs_2_ = bf16[32,2048]{1,0:T(8,128)(2,1)S(1)} collective-permute-done((bf16[32,2048]{1,0:T(8,128)(2,1)S(1)}, bf16[32,2048]{1,0:T(8,128)(2,1)S(1)}, u32[]{:S(2)}, u32[]{:S(2)}) %collective-permute-start.34) | collective-permute-done | bytes 131104 | tf_op jit(solution)/shard_map/ppermute | solution.py:406
  136.3 2.4 %collective-permute-done.40.refs_3_ = bf16[64,2048]{1,0:T(8,128)(2,1)S(1)} collective-permute-done((bf16[64,2048]{1,0:T(8,128)(2,1)S(1)}, bf16[64,2048]{1,0:T(8,128)(2,1)S(1)}, u32[]{:S(2)}, u32[]{:S(2)}) %collective-permute-start.40) | collective-permute-done | bytes 262176 | tf_op jit(solution)/shard_map/ppermute | solution.py:403
  138.7 8.3 %collective-permute-done.36.refs_2_ = bf16[64,2048]{1,0:T(8,128)(2,1)S(1)} collective-permute-done((bf16[64,2048]{1,0:T(8,128)(2,1)S(1)}, bf16[64,2048]{1,0:T(8,128)(2,1)S(1)}, u32[]{:S(2)}, u32[]{:S(2)}) %collective-permute-start.36) | collective-permute-done | bytes 262176 | tf_op jit(solution)/shard_map/ppermute | solution.py:403
  (75 shorter events, 49.1 us)
Async XLA Ops:
  0.0 86.6 %collective-permute-start.18 = (bf16[2048,1024]{1,0:T(8,128)(2,1)}, bf16[2048,1024]{1,0:T(8,128)(2,1)}, u32[]{:S(2)}, u32[]{:S(2)}) collective-permute-start(bf16[2048,1024]{1,0:T(8,128)(2,1)} %bitcast.8), channel_id=1, source_target_pairs={{0,1},{1,0},{2,3},{3,2},{4,5},{5,4},{6,7},{7,6},{8,9},{9,8},{10,11... | collective-permute-start | bytes 12582920 | tf_op jit(solution)/shard_map/ppermute | solution.py:394
  0.5 88.1 %collective-permute-start.19 = (bf16[2048,1024]{1,0:T(8,128)(2,1)}, bf16[2048,1024]{1,0:T(8,128)(2,1)}, u32[]{:S(2)}, u32[]{:S(2)}) collective-permute-start(bf16[2048,1024]{1,0:T(8,128)(2,1)} %bitcast.11), channel_id=1, source_target_pairs={{0,1},{1,0},{2,3},{3,2},{4,5},{5,4},{6,7},{7,6},{8,9},{9,8},{10,11... | collective-permute-start | bytes 12582920 | tf_op jit(solution)/shard_map/ppermute | solution.py:394
  0.5 89.3 %collective-permute-start.20 = (bf16[1024,2048]{1,0:T(8,128)(2,1)}, bf16[1024,2048]{1,0:T(8,128)(2,1)}, u32[]{:S(2)}, u32[]{:S(2)}) collective-permute-start(bf16[1024,2048]{1,0:T(8,128)(2,1)} %bitcast.14), channel_id=1, source_target_pairs={{0,1},{1,0},{2,3},{3,2},{4,5},{5,4},{6,7},{7,6},{8,9},{9,8},{10,11... | collective-permute-start | bytes 12582920 | tf_op jit(solution)/shard_map/ppermute | solution.py:394
  16.5 6.9 %collective-permute-start.4 = (bf16[136,256]{1,0:T(8,128)(2,1)S(1)}, bf16[136,256]{1,0:T(8,128)(2,1)S(1)}, u32[]{:S(2)}, u32[]{:S(2)}) collective-permute-start(bf16[136,256]{1,0:T(8,128)(2,1)S(1)} %shard_map.129.refs_4_), channel_id=1, source_target_pairs={{0,8},{2,10},{4,12},{6,14},{8,16},{10,18},{12,20},{14,22},{16,24},... | collective-permute-start | bytes 208904 | tf_op jit(solution)/shard_map/ppermute | solution.py:403
  27.8 7.3 %collective-permute-start.7 = (bf16[128,256]{1,0:T(8,128)(2,1)S(1)}, bf16[128,256]{1,0:T(8,128)(2,1)S(1)}, u32[]{:S(2)}, u32[]{:S(2)}) collective-permute-start(bf16[128,256]{1,0:T(8,128)(2,1)S(1)} %get-tuple-element.60), channel_id=1, source_target_pairs={{0,4},{2,6},{4,0},{6,2},{8,12},{10,14},{12,8},{14,10},{16,20},{18,... | collective-permute-start | bytes 196616 | tf_op jit(solution)/shard_map/ppermute | solution.py:406
  44.3 11.1 %collective-permute-start.11 = (bf16[64,2048]{1,0:T(8,128)(2,1)S(1)}, bf16[64,2048]{1,0:T(8,128)(2,1)S(1)}, u32[]{:S(2)}, u32[]{:S(2)}) collective-permute-start(bf16[64,2048]{1,0:T(8,128)(2,1)S(1)} %get-tuple-element.66.refs_0_), channel_id=1, source_target_pairs={{0,8},{2,10},{4,12},{6,14},{8,16},{10,18},{12,20},{14,22},{16,24},... | collective-permute-start | bytes 786440 | tf_op jit(solution)/shard_map/ppermute | solution.py:403
  48.4 11.8 %collective-permute-start.10 = (bf16[64,2048]{1,0:T(8,128)(2,1)S(1)}, bf16[64,2048]{1,0:T(8,128)(2,1)S(1)}, u32[]{:S(2)}, u32[]{:S(2)}) collective-permute-start(bf16[64,2048]{1,0:T(8,128)(2,1)S(1)} %get-tuple-element.66.refs_0_), channel_id=1, source_target_pairs={{0,24},{2,26},{4,28},{6,30},{8,0},{10,2},{12,4},{14,6},{16,8},{18,... | collective-permute-start | bytes 786440 | tf_op jit(solution)/shard_map/ppermute | solution.py:403
  61.7 7.7 %collective-permute-start.22 = (bf16[32,2048]{1,0:T(8,128)(2,1)S(1)}, bf16[32,2048]{1,0:T(8,128)(2,1)S(1)}, u32[]{:S(2)}, u32[]{:S(2)}) collective-permute-start(bf16[32,2048]{1,0:T(8,128)(2,1)S(1)} %get-tuple-element.76), channel_id=1, source_target_pairs={{0,24},{2,26},{4,28},{6,30},{8,0},{10,2},{12,4},{14,6},{16,8},{18,... | collective-permute-start | bytes 393224 | tf_op jit(solution)/shard_map/ppermute | solution.py:403
  66.9 7.4 %collective-permute-start.21 = (bf16[32,2048]{1,0:T(8,128)(2,1)S(1)}, bf16[32,2048]{1,0:T(8,128)(2,1)S(1)}, u32[]{:S(2)}, u32[]{:S(2)}) collective-permute-start(bf16[32,2048]{1,0:T(8,128)(2,1)S(1)} %get-tuple-element.68.refs_1_), channel_id=1, source_target_pairs={{0,8},{2,10},{4,12},{6,14},{8,16},{10,18},{12,20},{14,22},{16,24},... | collective-permute-start | bytes 393224 | tf_op jit(solution)/shard_map/ppermute | solution.py:403
  82.2 18.6 %collective-permute-start.31 = (bf16[32,2048]{1,0:T(8,128)(2,1)S(1)}, bf16[32,2048]{1,0:T(8,128)(2,1)S(1)}, u32[]{:S(2)}, u32[]{:S(2)}) collective-permute-start(bf16[32,2048]{1,0:T(8,128)(2,1)S(1)} %get-tuple-element.89), channel_id=1, source_target_pairs={{0,4},{2,6},{4,0},{6,2},{8,12},{10,14},{12,8},{14,10},{16,20},{18,... | collective-permute-start | bytes 393224 | tf_op jit(solution)/shard_map/ppermute | solution.py:406
  86.4 14.5 %collective-permute-start.32 = (bf16[32,2048]{1,0:T(8,128)(2,1)S(1)}, bf16[32,2048]{1,0:T(8,128)(2,1)S(1)}, u32[]{:S(2)}, u32[]{:S(2)}) collective-permute-start(bf16[32,2048]{1,0:T(8,128)(2,1)S(1)} %get-tuple-element.90), channel_id=1, source_target_pairs={{0,6},{2,4},{4,2},{6,0},{8,14},{10,12},{12,10},{14,8},{16,22},{18,... | collective-permute-start | bytes 393224 | tf_op jit(solution)/shard_map/ppermute | solution.py:406
  86.6 14.3 %collective-permute-start.27 = (bf16[32,2048]{1,0:T(8,128)(2,1)S(1)}, bf16[32,2048]{1,0:T(8,128)(2,1)S(1)}, u32[]{:S(2)}, u32[]{:S(2)}) collective-permute-start(bf16[32,2048]{1,0:T(8,128)(2,1)S(1)} %get-tuple-element.85), channel_id=1, source_target_pairs={{0,2},{2,0},{4,6},{6,4},{8,10},{10,8},{12,14},{14,12},{16,18},{18,... | collective-permute-start | bytes 393224 | tf_op jit(solution)/shard_map/ppermute | solution.py:406
  88.6 12.2 %collective-permute-start.28 = (bf16[32,2048]{1,0:T(8,128)(2,1)S(1)}, bf16[32,2048]{1,0:T(8,128)(2,1)S(1)}, u32[]{:S(2)}, u32[]{:S(2)}) collective-permute-start(bf16[32,2048]{1,0:T(8,128)(2,1)S(1)} %get-tuple-element.86), channel_id=1, source_target_pairs={{0,4},{2,6},{4,0},{6,2},{8,12},{10,14},{12,8},{14,10},{16,20},{18,... | collective-permute-start | bytes 393224 | tf_op jit(solution)/shard_map/ppermute | solution.py:406
  89.9 11.0 %collective-permute-start.29 = (bf16[32,2048]{1,0:T(8,128)(2,1)S(1)}, bf16[32,2048]{1,0:T(8,128)(2,1)S(1)}, u32[]{:S(2)}, u32[]{:S(2)}) collective-permute-start(bf16[32,2048]{1,0:T(8,128)(2,1)S(1)} %get-tuple-element.87), channel_id=1, source_target_pairs={{0,6},{2,4},{4,2},{6,0},{8,14},{10,12},{12,10},{14,8},{16,22},{18,... | collective-permute-start | bytes 393224 | tf_op jit(solution)/shard_map/ppermute | solution.py:406
  113.6 7.2 %collective-permute-start.37 = (bf16[32,2048]{1,0:T(8,128)(2,1)S(1)}, bf16[32,2048]{1,0:T(8,128)(2,1)S(1)}, u32[]{:S(2)}, u32[]{:S(2)}) collective-permute-start(bf16[32,2048]{1,0:T(8,128)(2,1)S(1)} %get-tuple-element.96), channel_id=1, source_target_pairs={{0,2},{2,0},{4,6},{6,4},{8,10},{10,8},{12,14},{14,12},{16,18},{18,... | collective-permute-start | bytes 393224 | tf_op jit(solution)/shard_map/ppermute | solution.py:406
  113.6 10.2 %collective-permute-start.38 = (bf16[32,2048]{1,0:T(8,128)(2,1)S(1)}, bf16[32,2048]{1,0:T(8,128)(2,1)S(1)}, u32[]{:S(2)}, u32[]{:S(2)}) collective-permute-start(bf16[32,2048]{1,0:T(8,128)(2,1)S(1)} %get-tuple-element.97), channel_id=1, source_target_pairs={{0,4},{2,6},{4,0},{6,2},{8,12},{10,14},{12,8},{14,10},{16,20},{18,... | collective-permute-start | bytes 393224 | tf_op jit(solution)/shard_map/ppermute | solution.py:406
  114.9 9.3 %collective-permute-start.39 = (bf16[32,2048]{1,0:T(8,128)(2,1)S(1)}, bf16[32,2048]{1,0:T(8,128)(2,1)S(1)}, u32[]{:S(2)}, u32[]{:S(2)}) collective-permute-start(bf16[32,2048]{1,0:T(8,128)(2,1)S(1)} %get-tuple-element.98), channel_id=1, source_target_pairs={{0,6},{2,4},{4,2},{6,0},{8,14},{10,12},{12,10},{14,8},{16,22},{18,... | collective-permute-start | bytes 393224 | tf_op jit(solution)/shard_map/ppermute | solution.py:406
  117.1 17.1 %collective-permute-start.23 = (bf16[64,2048]{1,0:T(8,128)(2,1)S(1)}, bf16[64,2048]{1,0:T(8,128)(2,1)S(1)}, u32[]{:S(2)}, u32[]{:S(2)}) collective-permute-start(bf16[64,2048]{1,0:T(8,128)(2,1)S(1)} %get-tuple-element.80), channel_id=1, source_target_pairs={{0,2},{2,0},{4,6},{6,4},{8,10},{10,8},{12,14},{14,12},{16,18},{18,... | collective-permute-start | bytes 786440 | tf_op jit(solution)/shard_map/ppermute | solution.py:406
  118.0 16.2 %collective-permute-start.24 = (bf16[64,2048]{1,0:T(8,128)(2,1)S(1)}, bf16[64,2048]{1,0:T(8,128)(2,1)S(1)}, u32[]{:S(2)}, u32[]{:S(2)}) collective-permute-start(bf16[64,2048]{1,0:T(8,128)(2,1)S(1)} %get-tuple-element.81), channel_id=1, source_target_pairs={{0,4},{2,6},{4,0},{6,2},{8,12},{10,14},{12,8},{14,10},{16,20},{18,... | collective-permute-start | bytes 786440 | tf_op jit(solution)/shard_map/ppermute | solution.py:406
  120.8 13.4 %collective-permute-start.25 = (bf16[64,2048]{1,0:T(8,128)(2,1)S(1)}, bf16[64,2048]{1,0:T(8,128)(2,1)S(1)}, u32[]{:S(2)}, u32[]{:S(2)}) collective-permute-start(bf16[64,2048]{1,0:T(8,128)(2,1)S(1)} %get-tuple-element.82), channel_id=1, source_target_pairs={{0,6},{2,4},{4,2},{6,0},{8,14},{10,12},{12,10},{14,8},{16,22},{18,... | collective-permute-start | bytes 786440 | tf_op jit(solution)/shard_map/ppermute | solution.py:406
  123.9 8.4 %collective-permute-start.34 = (bf16[32,2048]{1,0:T(8,128)(2,1)S(1)}, bf16[32,2048]{1,0:T(8,128)(2,1)S(1)}, u32[]{:S(2)}, u32[]{:S(2)}) collective-permute-start(bf16[32,2048]{1,0:T(8,128)(2,1)S(1)} %get-tuple-element.93), channel_id=1, source_target_pairs={{0,4},{2,6},{4,0},{6,2},{8,12},{10,14},{12,8},{14,10},{16,20},{18,... | collective-permute-start | bytes 393224 | tf_op jit(solution)/shard_map/ppermute | solution.py:406
  124.2 9.4 %collective-permute-start.35 = (bf16[32,2048]{1,0:T(8,128)(2,1)S(1)}, bf16[32,2048]{1,0:T(8,128)(2,1)S(1)}, u32[]{:S(2)}, u32[]{:S(2)}) collective-permute-start(bf16[32,2048]{1,0:T(8,128)(2,1)S(1)} %get-tuple-element.94), channel_id=1, source_target_pairs={{0,6},{2,4},{4,2},{6,0},{8,14},{10,12},{12,10},{14,8},{16,22},{18,... | collective-permute-start | bytes 393224 | tf_op jit(solution)/shard_map/ppermute | solution.py:406
  134.1 13.0 %collective-permute-start.36 = (bf16[64,2048]{1,0:T(8,128)(2,1)S(1)}, bf16[64,2048]{1,0:T(8,128)(2,1)S(1)}, u32[]{:S(2)}, u32[]{:S(2)}) collective-permute-start(bf16[64,2048]{1,0:T(8,128)(2,1)S(1)} %shard_map.141), channel_id=1, source_target_pairs={{0,16},{2,18},{4,20},{6,22},{8,24},{10,26},{12,28},{14,30},{16,0},... | collective-permute-start | bytes 786440 | tf_op jit(solution)/shard_map/ppermute | solution.py:403
  135.0 12.0 %collective-permute-start.26 = (bf16[64,2048]{1,0:T(8,128)(2,1)S(1)}, bf16[64,2048]{1,0:T(8,128)(2,1)S(1)}, u32[]{:S(2)}, u32[]{:S(2)}) collective-permute-start(bf16[64,2048]{1,0:T(8,128)(2,1)S(1)} %get-tuple-element.84), channel_id=1, source_target_pairs={{0,8},{2,10},{4,12},{6,14},{8,16},{10,18},{12,20},{14,22},{16,24},... | collective-permute-start | bytes 786440 | tf_op jit(solution)/shard_map/ppermute | solution.py:403
  (17 other events, 95.3 us)
where the time goes:
time: 148 us
  starting transfers between devices  56.4 us (38%)
  waiting for transfers between devices  55.8 us (38%)
  Pallas kernels  35.4 us (24%)
    pallas_call x17, Pallas kernels, placed(): run(*(spec.place(arg) for spec, arg in zip(specs, args, strict=True)))  35.4 us
    ppermute x27, starting transfers between devices, in_plane(): return lax.ppermute(part, 'sp', [(i, i ^ near) for i in range(sp)])  34.4 us
    ppermute x27, waiting for transfers between devices, in_plane(): return lax.ppermute(part, 'sp', [(i, i ^ near) for i in range(sp)])  27.6 us
    ppermute x10, waiting for transfers between devices, to_plane(): lax.ppermute(part, 'sp', [(i, (i + distance * inner) % sp) for i in range...  26.7 us
    ppermute x10, starting transfers between devices, to_plane(): lax.ppermute(part, 'sp', [(i, (i + distance * inner) % sp) for i in range...  21 us
  transfers between devices with their start and end apart: 41, of which 21 were waited for; matrix products, arithmetic and copies ran while one was open for 0% of the time, Pallas kernels for 16%

commit v1 on v0

--- a/solution.py
+++ b/solution.py
@@ -13,7 +13,6 @@
 EPS = 1e-05
 CLAMP_LIMIT = 7.0
 SIGMOID_SLOPE = 1.702
-HIDDEN = 512
 
 
 class Spec:
@@ -49,7 +48,7 @@
     ).astype(jnp.bfloat16)
 
 
-def state_kernel(me_ref, decay_ref, keys_ref, values_ref, *outs):
+def state_kernel(me_ref, _, decay_ref, keys_ref, values_ref, *outs):
     for near, out_ref in enumerate(outs):
         head = jnp.bitwise_xor(jnp.bitwise_and(me_ref[0], len(outs) - 1), near)
         out_ref[...] = head_state(keys_ref, values_ref, head, decay_ref[head])
@@ -106,7 +105,14 @@
         out_ref[...] = total.astype(jnp.bfloat16)
 
 
-def intra_kernel(decay_ref, q_ref, k_ref, v_ref, gate_ref, intra_ref, silu_ref):
+def intra_kernel(decay_ref, q_ref, k_ref, v_ref, gate_ref, *refs):
+    count = (len(refs) - 3) // 2
+    intra_ref, silu_ref, sems = refs[count], refs[count + 1], refs[-1]
+    copies = [
+        pltpu.make_async_copy(refs[i], refs[count + 2 + i], sems.at[i]) for i in range(count)
+    ]
+    for copy in copies:
+        copy.start()
     block_len = q_ref.shape[0]
     ahead = lax.broadcasted_iota(jnp.int32, (block_len, block_len), 0) - lax.broadcasted_iota(
         jnp.int32, (block_len, block_len), 1
@@ -128,6 +134,8 @@
         )
     gate = gate_ref[...].astype(jnp.float32)
     silu_ref[...] = gate / (1.0 + jnp.exp(-gate))
+    for copy in copies:
+        copy.wait()
 
 
 def mix_kernel(
@@ -137,22 +145,14 @@
     q_ref,
     intra_ref,
     silu_ref,
-    weight_hbm,
+    weight_ref,
     *refs,
 ):
     heads = decay_ref.shape[0]
-    states, (keep_ref, send_ref, state_ref, weight_ref, sems) = refs[:heads], refs[heads:]
+    states, (keep_ref, send_ref, state_ref) = refs[:heads], refs[heads:]
     plane = jnp.bitwise_and(me_ref[0], heads - 1)
     for near in range(heads):
         state_ref[near] = states[near][...]
-    copies = [
-        pltpu.make_async_copy(
-            weight_hbm.at[head_cols(h, DV)], weight_ref.at[head_cols(h, DV)], sems.at[h]
-        )
-        for h in range(heads)
-    ]
-    for copy in copies:
-        copy.start()
     block_len = q_ref.shape[0]
     lead = 1.0 + lax.broadcasted_iota(jnp.int32, (block_len, DV), 0).astype(jnp.float32)
     gated = []
@@ -167,7 +167,6 @@
         gated.append((normed * silu_ref[:, head_cols(h, DV)]).astype(jnp.bfloat16))
     total = jnp.zeros((block_len, weight_ref.shape[1]), jnp.float32)
     for h in range(heads):
-        copies[h].wait()
         total = total + jnp.dot(
             gated[h], weight_ref[head_cols(h, DV), :], preferred_element_type=jnp.float32
         )
@@ -294,55 +293,44 @@
     return jax.ShapeDtypeStruct(shape, jnp.bfloat16)
 
 
+def fetch_kernel(*refs):
+    count = (len(refs) - 1) // 2
+    copies = [
+        pltpu.make_async_copy(refs[i], refs[count + i], refs[-1].at[i]) for i in range(count)
+    ]
+    for copy in copies:
+        copy.start()
+    for copy in copies:
+        copy.wait()
+
+
+def fetch(arrays):
+    return call(
+        fetch_kernel,
+        tuple(bf16(*array.shape) for array in arrays),
+        [FAR] * len(arrays),
+        flops=1 << 32,
+        scratch=[pltpu.SemaphoreType.DMA((len(arrays),))],
+    )(*arrays)
+
+
 def expert_kernel(parts, gives, *refs):
     sources, weights, refs = refs[:parts], refs[parts : parts + 6], refs[parts + 6 :]
-    gate, lin, down, total, sems = refs[len(refs) - 5 :]
-    outs = refs[len(refs) - 5 - gives : len(refs) - 5]
-    slots, _, hidden = gate.shape
-    half = weights[0].shape[1] // hidden
-
-    def copies(at, source):
-        slot = lax.rem(at, slots)
-        block = pl.ds(pl.multiple_of(lax.rem(at, half) * hidden, hidden), hidden)
-        gate_hbm, lin_hbm, down_hbm = source
-        return (
-            pltpu.make_async_copy(gate_hbm.at[:, block], gate.at[slot], sems.at[0, slot]),
-            pltpu.make_async_copy(lin_hbm.at[:, block], lin.at[slot], sems.at[1, slot]),
-            pltpu.make_async_copy(down_hbm.at[block, :], down.at[slot], sems.at[2, slot]),
-        )
-
-    def start(at):
-        @pl.when(at < half)
-        def _():
-            for copy in copies(at, weights[:3]):
-                copy.start()
-
-        @pl.when(jnp.logical_and(at >= half, at < 2 * half))
-        def _():
-            for copy in copies(at, weights[3:]):
-                copy.start()
-
-    for at in range(slots - 1):
-        start(jnp.int32(at))
+    total = refs[-1]
+    outs = refs[len(refs) - 1 - gives : len(refs) - 1]
     rows = jnp.concatenate([source[...] for source in sources], axis=0)
-    total[...] = jnp.zeros_like(total)
-
-    def step(at, _):
-        start(at + slots - 1)
-        slot = lax.rem(at, slots)
-        arrive = copies(at, weights[:3])
-        arrive[0].wait()
-        pre = jnp.dot(rows, gate[slot], preferred_element_type=jnp.float32)
+    for part in range(2):
+        gate, lin, down = weights[3 * part : 3 * part + 3]
+        pre = jnp.dot(rows, gate[...], preferred_element_type=jnp.float32)
         clipped = jnp.minimum(pre, CLAMP_LIMIT)
         act = clipped / (1.0 + jnp.exp(-SIGMOID_SLOPE * clipped))
-        arrive[1].wait()
-        pre = jnp.dot(rows, lin[slot], preferred_element_type=jnp.float32)
+        pre = jnp.dot(rows, lin[...], preferred_element_type=jnp.float32)
         act = (act * (jnp.clip(pre, -CLAMP_LIMIT, CLAMP_LIMIT) + 1.0)).astype(jnp.bfloat16)
-        arrive[2].wait()
-        total[...] += jnp.dot(act, down[slot], preferred_element_type=jnp.float32)
-        return 0
-
-    lax.fori_loop(0, 2 * half, step, 0)
+        more = jnp.dot(act, down[...], preferred_element_type=jnp.float32)
+        if part == 0:
+            total[...] = more
+        else:
+            total[...] += more
     at = 0
     for out_ref in outs:
         each = out_ref.shape[0]
@@ -350,21 +338,15 @@
         at += each
 
 
-def run_experts(sources, gives, own, other, after, hidden=HIDDEN, slots=2):
+def run_experts(sources, gives, own, other, after):
     count, width = sum(source.shape[0] for source in sources), sources[0].shape[1]
     run = call(
         functools.partial(expert_kernel, len(sources), gives),
         tuple(bf16(count // gives, width) for _ in range(gives)),
-        [NEAR] * len(sources) + [FAR] * 6 + [AFTER] * len(after),
+        [NEAR] * (len(sources) + 6) + [AFTER] * len(after),
         flops=12 * count * width * own[0].shape[1],
-        mib=40,
-        scratch=[
-            pltpu.VMEM((slots, width, hidden), jnp.bfloat16),
-            pltpu.VMEM((slots, width, hidden), jnp.bfloat16),
-            pltpu.VMEM((slots, hidden, width), jnp.bfloat16),
-            pltpu.VMEM((count, width), jnp.float32),
-            pltpu.SemaphoreType.DMA((3, slots)),
-        ],
+        mib=24,
+        scratch=[pltpu.VMEM((count, width), jnp.float32)],
     )
     return run(*sources, *own, *other, *after)
 
@@ -392,7 +374,8 @@
     swap = [(i, (i + 1) % tp) for i in range(tp)]
     mine = (gate_up[0], lin_up[0], down_weight[0])
     other = [lax.ppermute(part, "tp", swap) for part in mine]
-    me = lax.axis_index("sp").reshape(1)
+    held, swapped = mine, fetch(other)
+    me, half_of = lax.axis_index("sp").reshape(1), lax.axis_index("tp").reshape(1)
 
     inner = heads
     outer = sp // inner
@@ -406,8 +389,8 @@
         return lax.ppermute(part, "sp", [(i, i ^ near) for i in range(sp)])
 
     near_chips = range(1, inner)
-    sums = call(state_kernel, (bf16(DK, DV),) * inner, [SCALAR, SMEM, VMEM, VMEM])(
-        me, decay_rate, keys, values
+    sums = call(state_kernel, (bf16(DK, DV),) * inner, [SCALAR, SCALAR, SMEM, VMEM, VMEM])(
+        me, half_of, decay_rate, keys, values
     )
     sums = [sums[0]] + [in_plane(sums[r], r) for r in near_chips]
     total = call(
@@ -423,24 +406,24 @@
     carried = [carried[0]] + [in_plane(carried[r], r) for r in near_chips]
 
     term = jax.ShapeDtypeStruct((block_len, heads * DV), jnp.float32)
-    intra, silu = call(intra_kernel, (term, term), [SMEM] + [VMEM] * 4, flops=1 << 32)(
-        decay_rate, queries, keys, values, out_gate
-    )
+    gain = ffn_gain.reshape(1, width)
+    intra, silu, weight, near_residual, near_gain = call(
+        intra_kernel,
+        (term, term, bf16(*out_weight.shape), bf16(own_rows, width), gain),
+        [SMEM] + [VMEM] * 4 + [FAR] * 3,
+        flops=1 << 32,
+        scratch=[pltpu.SemaphoreType.DMA((3,))],
+    )(decay_rate, queries, keys, values, out_gate, out_weight, residual, gain)
     keep, send = call(
         mix_kernel,
         (bf16(own_rows, width), bf16(own_rows, width)),
-        [SCALAR, SMEM, SCALAR, VMEM, NEAR, NEAR, FAR] + [NEAR] * inner,
-        mib=16,
-        scratch=[
-            pltpu.VMEM((heads, DK, DV), jnp.bfloat16),
-            pltpu.VMEM(out_weight.shape, jnp.bfloat16),
-            pltpu.SemaphoreType.DMA((heads,)),
-        ],
-    )(me, decay_rate, lax.axis_index("tp").reshape(1), queries, intra, silu, out_weight, *carried)
+        [SCALAR, SMEM, SCALAR, VMEM] + [NEAR] * (3 + inner),
+        scratch=[pltpu.VMEM((heads, DK, DV), jnp.bfloat16)],
+    )(me, decay_rate, half_of, queries, intra, silu, weight, *carried)
     got = lax.ppermute(send, "tp", swap)
-    mixed, rows = call(
-        norm_kernel, (bf16(own_rows, width), bf16(own_rows, width)), [VMEM, NEAR, NEAR, VMEM]
-    )(residual, keep, got, ffn_gain.reshape(1, width))
+    mixed, rows = call(norm_kernel, (bf16(own_rows, width), bf16(own_rows, width)), [NEAR] * 4)(
+        near_residual, keep, got, near_gain
+    )
 
     size = max(1, outer // 4)
     groups = [range(i, min(i + size, outer)) for i in range(0, outer, size)]
@@ -484,9 +467,9 @@
 
     half = (len(groups) + 1) // 2
     first = [slots[r] for r in range(inner) for slots in sent[:half]]
-    early = run_experts(first, inner, mine, other, after)
+    early = run_experts(first, inner, held, swapped, after)
     second = [slots[r] for slots in reversed(sent[half:]) for r in range(inner)]
-    late = run_experts(second, len(second), mine, other, early[:1])
+    late = run_experts(second, len(second), held, swapped, early[:1])
     home = send_home([n for places in groups[:half] for n in places], early)
     for g, places in enumerate(reversed(groups[half:])):
         home += send_home(places, late[g * inner : (g + 1) * inner])

time: 148 us -> 139 us (0.939)
  waiting for transfers between devices: 55.8 us -> 48.2 us
  Pallas kernels: 35.4 us -> 31.9 us
  starting transfers between devices: 56.4 us -> 58.3 us
    ppermute x27, waiting for transfers between devices: 27.6 us -> 19.2 us  [in_plane(): return lax.ppermute(part, 'sp', [(i, i ^ near) for i in range(sp)])]
    pallas_call x17 -> x18, Pallas kernels: 35.4 us -> 31.9 us  [placed(): run(*(spec.place(arg) for spec, arg in zip(specs, args, strict=True)))]
  transfers between devices with their start and end apart: 41 -> 41, of which waited for: 21 -> 16; matrix products, arithmetic and copies ran while one was open for 0% -> 0% of each run, Pallas kernels for 16% -> 17%
where the time goes in v1:
time: 139 us
  starting transfers between devices  58.3 us (42%)
  waiting for transfers between devices  48.2 us (35%)
  Pallas kernels  31.9 us (23%)
    ppermute x27, starting transfers between devices, in_plane(): return lax.ppermute(part, 'sp', [(i, i ^ near) for i in range(sp)])  35.4 us
    pallas_call x18, Pallas kernels, placed(): run(*(spec.place(arg) for spec, arg in zip(specs, args, strict=True)))  31.9 us
    ppermute x10, waiting for transfers between devices, to_plane(): lax.ppermute(part, 'sp', [(i, (i + distance * inner) % sp) for i in range...  27.4 us
    ppermute x10, starting transfers between devices, to_plane(): lax.ppermute(part, 'sp', [(i, (i + distance * inner) % sp) for i in range...  21.8 us
    ppermute x27, waiting for transfers between devices, in_plane(): return lax.ppermute(part, 'sp', [(i, i ^ near) for i in range(sp)])  19.2 us
  transfers between devices with their start and end apart: 41, of which 16 were waited for; matrix products, arithmetic and copies ran while one was open for 0% of the time, Pallas kernels for 17%

profile of v1, /device:TPU:0, one launch (start us, length us, event | category | flops | bytes accessed | tf_op | source)
XLA Modules:
  0.0 138.6 jit_solution(16811704857718552621)
XLA Ops:
  2.3 2.5 %collective-permute-start = (bf16[128,256]{1,0:T(8,128)(2,1)S(1)}, bf16[128,256]{1,0:T(8,128)(2,1)S(1)}, u32[]{:S(2)}, u32[]{:S(2)}) collective-permute-start(bf16[128,256]{1,0:T(8,128)(2,1)S(1)} %get-tuple-element.63), channel_id=1, source_target_pairs={{0,2},{2,0},{4,6},{6,4},{8,10},{10,8},{12,14},{14,12},{16,18},{18,... | collective-permute-start | bytes 196616 | tf_op jit(solution)/shard_map/ppermute | solution.py:389
  7.6 2.7 %collective-permute-start.2 = (bf16[128,256]{1,0:T(8,128)(2,1)S(1)}, bf16[128,256]{1,0:T(8,128)(2,1)S(1)}, u32[]{:S(2)}, u32[]{:S(2)}) collective-permute-start(bf16[128,256]{1,0:T(8,128)(2,1)S(1)} %get-tuple-element.65), channel_id=1, source_target_pairs={{0,6},{2,4},{4,2},{6,0},{8,14},{10,12},{12,10},{14,8},{16,22},{18,... | collective-permute-start | bytes 196616 | tf_op jit(solution)/shard_map/ppermute | solution.py:389
  10.3 2.5 %collective-permute-done.2.refs_3_ = bf16[128,256]{1,0:T(8,128)(2,1)S(1)} collective-permute-done((bf16[128,256]{1,0:T(8,128)(2,1)S(1)}, bf16[128,256]{1,0:T(8,128)(2,1)S(1)}, u32[]{:S(2)}, u32[]{:S(2)}) %collective-permute-start.2) | collective-permute-done | bytes 65568 | tf_op jit(solution)/shard_map/ppermute | solution.py:389
  13.6 2.8 %collective-permute-start.5 = (bf16[136,256]{1,0:T(8,128)(2,1)S(1)}, bf16[136,256]{1,0:T(8,128)(2,1)S(1)}, u32[]{:S(2)}, u32[]{:S(2)}) collective-permute-start(bf16[136,256]{1,0:T(8,128)(2,1)S(1)} %shard_map.129.refs_4_), channel_id=1, source_target_pairs={{0,16},{2,18},{4,20},{6,22},{8,24},{10,26},{12,28},{14,30},{16,0},... | collective-permute-start | bytes 208904 | tf_op jit(solution)/shard_map/ppermute | solution.py:386
  18.9 4.5 %collective-permute-start.3 = (bf16[136,256]{1,0:T(8,128)(2,1)S(1)}, bf16[136,256]{1,0:T(8,128)(2,1)S(1)}, u32[]{:S(2)}, u32[]{:S(2)}) collective-permute-start(bf16[136,256]{1,0:T(8,128)(2,1)S(1)} %shard_map.129.refs_4_), channel_id=1, source_target_pairs={{0,24},{2,26},{4,28},{6,30},{8,0},{10,2},{12,4},{14,6},{16,8},{18,... | collective-permute-start | bytes 208904 | tf_op jit(solution)/shard_map/ppermute | solution.py:386
  23.3 1.9 %collective-permute-done.3.refs_5_ = bf16[136,256]{1,0:T(8,128)(2,1)S(1)} collective-permute-done((bf16[136,256]{1,0:T(8,128)(2,1)S(1)}, bf16[136,256]{1,0:T(8,128)(2,1)S(1)}, u32[]{:S(2)}, u32[]{:S(2)}) %collective-permute-start.3) | collective-permute-done | bytes 69664 | tf_op jit(solution)/shard_map/ppermute | solution.py:386
  30.9 2.1 %collective-permute-start.8 = (bf16[128,256]{1,0:T(8,128)(2,1)S(1)}, bf16[128,256]{1,0:T(8,128)(2,1)S(1)}, u32[]{:S(2)}, u32[]{:S(2)}) collective-permute-start(bf16[128,256]{1,0:T(8,128)(2,1)S(1)} %get-tuple-element.69), channel_id=1, source_target_pairs={{0,6},{2,4},{4,2},{6,0},{8,14},{10,12},{12,10},{14,8},{16,22},{18,... | collective-permute-start | bytes 196616 | tf_op jit(solution)/shard_map/ppermute | solution.py:389
  33.0 3.4 %shard_map.127 = (f32[128,1024]{1,0:T(8,128)S(1)}, f32[128,1024]{1,0:T(8,128)S(1)}, bf16[1024,2048]{1,0:T(8,128)(2,1)S(1)}, bf16[64,2048]{1,0:T(8,128)(2,1)S(1)}, f32[1,2048]{1,0:T(1,128)S(1)}) custom-call(f32[4]{0:T(128)} %decay_ref.9, bf16[128,512]{1,0:T(8,128)(2,1)} %q_ref.3, bf16[128,512]{1,0:T(8,128)(2,1)} %keys_ref.1, bf16[128,1024]{1,0:T(8,128)(2,1)} %values_ref.1, ...), custom_call_target="tpu_custom_call" | custom-call | flops 4294967296 | bytes 1048576 | tf_op jit(solution)/shard_map/pallas_call | solution.py:287
  36.5 1.9 %shard_map.131 = (bf16[64,2048]{1,0:T(8,128)(2,1)S(1)}, bf16[64,2048]{1,0:T(8,128)(2,1)S(1)}) custom-call(s32[1]{0:T(128)} %bitcast.1.me_ref, f32[4]{0:T(128)} %decay_ref.9, s32[1]{0:T(128)} %bitcast.2._.tp_ref, bf16[128,512]{1,0:T(8,128)(2,1)} %q_ref.3, f32[128,1024]{1,0:T(8,128)S(1)} %get-tuple-element.59.intra_ref, ...), custom_call_target="tpu_custom_call" | custom-call | flops 268435456 | bytes 1048576 | tf_op jit(solution)/shard_map/pallas_call | solution.py:287
  40.5 4.0 %collective-permute-start.10 = (bf16[64,2048]{1,0:T(8,128)(2,1)S(1)}, bf16[64,2048]{1,0:T(8,128)(2,1)S(1)}, u32[]{:S(2)}, u32[]{:S(2)}) collective-permute-start(bf16[64,2048]{1,0:T(8,128)(2,1)S(1)} %get-tuple-element.75.refs_0_), channel_id=1, source_target_pairs={{0,24},{2,26},{4,28},{6,30},{8,0},{10,2},{12,4},{14,6},{16,8},{18,... | collective-permute-start | bytes 786440 | tf_op jit(solution)/shard_map/ppermute | solution.py:386
  44.9 6.7 %collective-permute-done.11.low_ref.refs_0_ = bf16[64,2048]{1,0:T(8,128)(2,1)S(1)} collective-permute-done((bf16[64,2048]{1,0:T(8,128)(2,1)S(1)}, bf16[64,2048]{1,0:T(8,128)(2,1)S(1)}, u32[]{:S(2)}, u32[]{:S(2)}) %collective-permute-start.11) | collective-permute-done | bytes 262176 | tf_op jit(solution)/shard_map/ppermute | solution.py:386
  51.7 2.7 %collective-permute-done.10.high_ref.refs_0_ = bf16[64,2048]{1,0:T(8,128)(2,1)S(1)} collective-permute-done((bf16[64,2048]{1,0:T(8,128)(2,1)S(1)}, bf16[64,2048]{1,0:T(8,128)(2,1)S(1)}, u32[]{:S(2)}, u32[]{:S(2)}) %collective-permute-start.10) | collective-permute-done | bytes 262176 | tf_op jit(solution)/shard_map/ppermute | solution.py:386
  54.4 4.2 %collective-permute-start.22 = (bf16[32,2048]{1,0:T(8,128)(2,1)S(1)}, bf16[32,2048]{1,0:T(8,128)(2,1)S(1)}, u32[]{:S(2)}, u32[]{:S(2)}) collective-permute-start(bf16[32,2048]{1,0:T(8,128)(2,1)S(1)} %get-tuple-element.88), channel_id=1, source_target_pairs={{0,24},{2,26},{4,28},{6,30},{8,0},{10,2},{12,4},{14,6},{16,8},{18,... | collective-permute-start | bytes 393224 | tf_op jit(solution)/shard_map/ppermute | solution.py:386
  58.5 3.6 %collective-permute-done.22.refs_1_ = bf16[32,2048]{1,0:T(8,128)(2,1)S(1)} collective-permute-done((bf16[32,2048]{1,0:T(8,128)(2,1)S(1)}, bf16[32,2048]{1,0:T(8,128)(2,1)S(1)}, u32[]{:S(2)}, u32[]{:S(2)}) %collective-permute-start.22) | collective-permute-done | bytes 131104 | tf_op jit(solution)/shard_map/ppermute | solution.py:386
  62.9 2.3 %collective-permute-done.21.refs_0_ = bf16[32,2048]{1,0:T(8,128)(2,1)S(1)} collective-permute-done((bf16[32,2048]{1,0:T(8,128)(2,1)S(1)}, bf16[32,2048]{1,0:T(8,128)(2,1)S(1)}, u32[]{:S(2)}, u32[]{:S(2)}) %collective-permute-start.21) | collective-permute-done | bytes 131104 | tf_op jit(solution)/shard_map/ppermute | solution.py:386
  68.9 6.3 %collective-permute-done.14.refs_4_ = bf16[32,2048]{1,0:T(8,128)(2,1)S(1)} collective-permute-done((bf16[32,2048]{1,0:T(8,128)(2,1)S(1)}, bf16[32,2048]{1,0:T(8,128)(2,1)S(1)}, u32[]{:S(2)}, u32[]{:S(2)}) %collective-permute-start.14) | collective-permute-done | bytes 131104 | tf_op jit(solution)/shard_map/ppermute | solution.py:389
  79.5 5.1 %shard_map.136 = (bf16[2048,1024]{1,0:T(8,128)(2,1)S(1)}, bf16[2048,1024]{1,0:T(8,128)(2,1)S(1)}, bf16[1024,2048]{1,0:T(8,128)(2,1)S(1)}) custom-call(bf16[2048,1024]{1,0:T(8,128)(2,1)} %collective-permute-done.18.refs_0_, bf16[2048,1024]{1,0:T(8,128)(2,1)} %collective-permute-done.19.refs_1_, bf16[1024,2048]{1,0:T(8,128)(2,1)} %collective-permute-done.20.refs_2_), custom_call_target="tpu_custom_call" | custom-call | flops 4294967296 | bytes 1048576 | tf_op jit(solution)/shard_map/pallas_call | solution.py:287
  84.6 1.6 %collective-permute-start.31 = (bf16[32,2048]{1,0:T(8,128)(2,1)S(1)}, bf16[32,2048]{1,0:T(8,128)(2,1)S(1)}, u32[]{:S(2)}, u32[]{:S(2)}) collective-permute-start(bf16[32,2048]{1,0:T(8,128)(2,1)S(1)} %get-tuple-element.101), channel_id=1, source_target_pairs={{0,4},{2,6},{4,0},{6,2},{8,12},{10,14},{12,8},{14,10},{16,20},{18,... | collective-permute-start | bytes 393224 | tf_op jit(solution)/shard_map/ppermute | solution.py:389
  91.1 6.8 %shard_map.139 = (bf16[64,2048]{1,0:T(8,128)(2,1)S(1)}, bf16[64,2048]{1,0:T(8,128)(2,1)S(1)}, bf16[64,2048]{1,0:T(8,128)(2,1)S(1)}, bf16[64,2048]{1,0:T(8,128)(2,1)S(1)}) custom-call(bf16[32,2048]{1,0:T(8,128)(2,1)S(1)} %get-tuple-element.76.refs_0_, bf16[32,2048]{1,0:T(8,128)(2,1)S(1)} %get-tuple-element.78.refs_1_, ...), custom_call_target="tpu_custom_call" | custom-call | flops 6442450944 | bytes 1048576 | tf_op jit(solution)/shard_map/pallas_call | solution.py:287
  98.0 7.1 %shard_map.141 = (bf16[32,2048]{1,0:T(8,128)(2,1)S(1)}, bf16[32,2048]{1,0:T(8,128)(2,1)S(1)}, bf16[32,2048]{1,0:T(8,128)(2,1)S(1)}, bf16[32,2048]{1,0:T(8,128)(2...) custom-call(bf16[32,2048]{1,0:T(8,128)(2,1)S(1)} %get-tuple-element., ...), custom_call_target="tpu_custom_call" | custom-call | flops 6442450944 | bytes 1048576 | tf_op jit(solution)/shard_map/pallas_call | solution.py:287
  107.3 1.9 %collective-permute-start.39 = (bf16[32,2048]{1,0:T(8,128)(2,1)S(1)}, bf16[32,2048]{1,0:T(8,128)(2,1)S(1)}, u32[]{:S(2)}, u32[]{:S(2)}) collective-permute-start(bf16[32,2048]{1,0:T(8,128)(2,1)S(1)} %get-tuple-element.110), channel_id=1, source_target_pairs={{0,6},{2,4},{4,2},{6,0},{8,14},{10,12},{12,10},{14,8},{16,22},{18,... | collective-permute-start | bytes 393224 | tf_op jit(solution)/shard_map/ppermute | solution.py:389
  116.0 6.5 %collective-permute-done.34.refs_2_ = bf16[32,2048]{1,0:T(8,128)(2,1)S(1)} collective-permute-done((bf16[32,2048]{1,0:T(8,128)(2,1)S(1)}, bf16[32,2048]{1,0:T(8,128)(2,1)S(1)}, u32[]{:S(2)}, u32[]{:S(2)}) %collective-permute-start.34) | collective-permute-done | bytes 131104 | tf_op jit(solution)/shard_map/ppermute | solution.py:389
  126.3 2.1 %collective-permute-start.26 = (bf16[64,2048]{1,0:T(8,128)(2,1)S(1)}, bf16[64,2048]{1,0:T(8,128)(2,1)S(1)}, u32[]{:S(2)}, u32[]{:S(2)}) collective-permute-start(bf16[64,2048]{1,0:T(8,128)(2,1)S(1)} %get-tuple-element.96), channel_id=1, source_target_pairs={{0,8},{2,10},{4,12},{6,14},{8,16},{10,18},{12,20},{14,22},{16,24},... | collective-permute-start | bytes 786440 | tf_op jit(solution)/shard_map/ppermute | solution.py:386
  129.0 8.7 %collective-permute-done.36.refs_2_ = bf16[64,2048]{1,0:T(8,128)(2,1)S(1)} collective-permute-done((bf16[64,2048]{1,0:T(8,128)(2,1)S(1)}, bf16[64,2048]{1,0:T(8,128)(2,1)S(1)}, u32[]{:S(2)}, u32[]{:S(2)}) %collective-permute-start.36) | collective-permute-done | bytes 262176 | tf_op jit(solution)/shard_map/ppermute | solution.py:386
  (82 shorter events, 44.3 us)
Async XLA Ops:
  0.0 75.9 %collective-permute-start.18 = (bf16[2048,1024]{1,0:T(8,128)(2,1)}, bf16[2048,1024]{1,0:T(8,128)(2,1)}, u32[]{:S(2)}, u32[]{:S(2)}) collective-permute-start(bf16[2048,1024]{1,0:T(8,128)(2,1)} %bitcast.8), channel_id=1, source_target_pairs={{0,1},{1,0},{2,3},{3,2},{4,5},{5,4},{6,7},{7,6},{8,9},{9,8},{10,11... | collective-permute-start | bytes 12582920 | tf_op jit(solution)/shard_map/ppermute | solution.py:376
  0.5 76.6 %collective-permute-start.19 = (bf16[2048,1024]{1,0:T(8,128)(2,1)}, bf16[2048,1024]{1,0:T(8,128)(2,1)}, u32[]{:S(2)}, u32[]{:S(2)}) collective-permute-start(bf16[2048,1024]{1,0:T(8,128)(2,1)} %bitcast.11), channel_id=1, source_target_pairs={{0,1},{1,0},{2,3},{3,2},{4,5},{5,4},{6,7},{7,6},{8,9},{9,8},{10,11... | collective-permute-start | bytes 12582920 | tf_op jit(solution)/shard_map/ppermute | solution.py:376
  0.5 78.1 %collective-permute-start.20 = (bf16[1024,2048]{1,0:T(8,128)(2,1)}, bf16[1024,2048]{1,0:T(8,128)(2,1)}, u32[]{:S(2)}, u32[]{:S(2)}) collective-permute-start(bf16[1024,2048]{1,0:T(8,128)(2,1)} %bitcast.14), channel_id=1, source_target_pairs={{0,1},{1,0},{2,3},{3,2},{4,5},{5,4},{6,7},{7,6},{8,9},{9,8},{10,11... | collective-permute-start | bytes 12582920 | tf_op jit(solution)/shard_map/ppermute | solution.py:376
  27.8 8.6 %collective-permute-start.7 = (bf16[128,256]{1,0:T(8,128)(2,1)S(1)}, bf16[128,256]{1,0:T(8,128)(2,1)S(1)}, u32[]{:S(2)}, u32[]{:S(2)}) collective-permute-start(bf16[128,256]{1,0:T(8,128)(2,1)S(1)} %get-tuple-element.68), channel_id=1, source_target_pairs={{0,4},{2,6},{4,0},{6,2},{8,12},{10,14},{12,8},{14,10},{16,20},{18,... | collective-permute-start | bytes 196616 | tf_op jit(solution)/shard_map/ppermute | solution.py:389
  40.3 11.4 %collective-permute-start.11 = (bf16[64,2048]{1,0:T(8,128)(2,1)S(1)}, bf16[64,2048]{1,0:T(8,128)(2,1)S(1)}, u32[]{:S(2)}, u32[]{:S(2)}) collective-permute-start(bf16[64,2048]{1,0:T(8,128)(2,1)S(1)} %get-tuple-element.75.refs_0_), channel_id=1, source_target_pairs={{0,8},{2,10},{4,12},{6,14},{8,16},{10,18},{12,20},{14,22},{16,24},... | collective-permute-start | bytes 786440 | tf_op jit(solution)/shard_map/ppermute | solution.py:386
  40.5 13.8 %collective-permute-start.10 = (bf16[64,2048]{1,0:T(8,128)(2,1)S(1)}, bf16[64,2048]{1,0:T(8,128)(2,1)S(1)}, u32[]{:S(2)}, u32[]{:S(2)}) collective-permute-start(bf16[64,2048]{1,0:T(8,128)(2,1)S(1)} %get-tuple-element.75.refs_0_), channel_id=1, source_target_pairs={{0,24},{2,26},{4,28},{6,30},{8,0},{10,2},{12,4},{14,6},{16,8},{18,... | collective-permute-start | bytes 786440 | tf_op jit(solution)/shard_map/ppermute | solution.py:386
  65.3 9.9 %collective-permute-start.14 = (bf16[32,2048]{1,0:T(8,128)(2,1)S(1)}, bf16[32,2048]{1,0:T(8,128)(2,1)S(1)}, u32[]{:S(2)}, u32[]{:S(2)}) collective-permute-start(bf16[32,2048]{1,0:T(8,128)(2,1)S(1)} %get-tuple-element.81), channel_id=1, source_target_pairs={{0,4},{2,6},{4,0},{6,2},{8,12},{10,14},{12,8},{14,10},{16,20},{18,... | collective-permute-start | bytes 393224 | tf_op jit(solution)/shard_map/ppermute | solution.py:389
  67.3 17.3 %collective-permute-start.16 = (bf16[32,2048]{1,0:T(8,128)(2,1)S(1)}, bf16[32,2048]{1,0:T(8,128)(2,1)S(1)}, u32[]{:S(2)}, u32[]{:S(2)}) collective-permute-start(bf16[32,2048]{1,0:T(8,128)(2,1)S(1)} %get-tuple-element.83), channel_id=1, source_target_pairs={{0,6},{2,4},{4,2},{6,0},{8,14},{10,12},{12,10},{14,8},{16,22},{18,... | collective-permute-start | bytes 393224 | tf_op jit(solution)/shard_map/ppermute | solution.py:389
  75.2 11.1 %collective-permute-start.13 = (bf16[32,2048]{1,0:T(8,128)(2,1)S(1)}, bf16[32,2048]{1,0:T(8,128)(2,1)S(1)}, u32[]{:S(2)}, u32[]{:S(2)}) collective-permute-start(bf16[32,2048]{1,0:T(8,128)(2,1)S(1)} %get-tuple-element.80), channel_id=1, source_target_pairs={{0,2},{2,0},{4,6},{6,4},{8,10},{10,8},{12,14},{14,12},{16,18},{18,... | collective-permute-start | bytes 393224 | tf_op jit(solution)/shard_map/ppermute | solution.py:389
  75.9 11.6 %collective-permute-start.15 = (bf16[32,2048]{1,0:T(8,128)(2,1)S(1)}, bf16[32,2048]{1,0:T(8,128)(2,1)S(1)}, u32[]{:S(2)}, u32[]{:S(2)}) collective-permute-start(bf16[32,2048]{1,0:T(8,128)(2,1)S(1)} %get-tuple-element.82), channel_id=1, source_target_pairs={{0,4},{2,6},{4,0},{6,2},{8,12},{10,14},{12,8},{14,10},{16,20},{18,... | collective-permute-start | bytes 393224 | tf_op jit(solution)/shard_map/ppermute | solution.py:389
  77.1 11.0 %collective-permute-start.17 = (bf16[32,2048]{1,0:T(8,128)(2,1)S(1)}, bf16[32,2048]{1,0:T(8,128)(2,1)S(1)}, u32[]{:S(2)}, u32[]{:S(2)}) collective-permute-start(bf16[32,2048]{1,0:T(8,128)(2,1)S(1)} %get-tuple-element.84), channel_id=1, source_target_pairs={{0,6},{2,4},{4,2},{6,0},{8,14},{10,12},{12,10},{14,8},{16,22},{18,... | collective-permute-start | bytes 393224 | tf_op jit(solution)/shard_map/ppermute | solution.py:389
  78.7 11.1 %collective-permute-start.30 = (bf16[32,2048]{1,0:T(8,128)(2,1)S(1)}, bf16[32,2048]{1,0:T(8,128)(2,1)S(1)}, u32[]{:S(2)}, u32[]{:S(2)}) collective-permute-start(bf16[32,2048]{1,0:T(8,128)(2,1)S(1)} %get-tuple-element.100), channel_id=1, source_target_pairs={{0,2},{2,0},{4,6},{6,4},{8,10},{10,8},{12,14},{14,12},{16,18},{18,... | collective-permute-start | bytes 393224 | tf_op jit(solution)/shard_map/ppermute | solution.py:389
  84.6 13.3 %collective-permute-start.31 = (bf16[32,2048]{1,0:T(8,128)(2,1)S(1)}, bf16[32,2048]{1,0:T(8,128)(2,1)S(1)}, u32[]{:S(2)}, u32[]{:S(2)}) collective-permute-start(bf16[32,2048]{1,0:T(8,128)(2,1)S(1)} %get-tuple-element.101), channel_id=1, source_target_pairs={{0,4},{2,6},{4,0},{6,2},{8,12},{10,14},{12,8},{14,10},{16,20},{18,... | collective-permute-start | bytes 393224 | tf_op jit(solution)/shard_map/ppermute | solution.py:389
  86.2 11.7 %collective-permute-start.32 = (bf16[32,2048]{1,0:T(8,128)(2,1)S(1)}, bf16[32,2048]{1,0:T(8,128)(2,1)S(1)}, u32[]{:S(2)}, u32[]{:S(2)}) collective-permute-start(bf16[32,2048]{1,0:T(8,128)(2,1)S(1)} %get-tuple-element.102), channel_id=1, source_target_pairs={{0,6},{2,4},{4,2},{6,0},{8,14},{10,12},{12,10},{14,8},{16,22},{18,... | collective-permute-start | bytes 393224 | tf_op jit(solution)/shard_map/ppermute | solution.py:389
  87.6 10.3 %collective-permute-start.27 = (bf16[32,2048]{1,0:T(8,128)(2,1)S(1)}, bf16[32,2048]{1,0:T(8,128)(2,1)S(1)}, u32[]{:S(2)}, u32[]{:S(2)}) collective-permute-start(bf16[32,2048]{1,0:T(8,128)(2,1)S(1)} %get-tuple-element.97), channel_id=1, source_target_pairs={{0,2},{2,0},{4,6},{6,4},{8,10},{10,8},{12,14},{14,12},{16,18},{18,... | collective-permute-start | bytes 393224 | tf_op jit(solution)/shard_map/ppermute | solution.py:389
  88.2 9.8 %collective-permute-start.28 = (bf16[32,2048]{1,0:T(8,128)(2,1)S(1)}, bf16[32,2048]{1,0:T(8,128)(2,1)S(1)}, u32[]{:S(2)}, u32[]{:S(2)}) collective-permute-start(bf16[32,2048]{1,0:T(8,128)(2,1)S(1)} %get-tuple-element.98), channel_id=1, source_target_pairs={{0,4},{2,6},{4,0},{6,2},{8,12},{10,14},{12,8},{14,10},{16,20},{18,... | collective-permute-start | bytes 393224 | tf_op jit(solution)/shard_map/ppermute | solution.py:389
  89.7 8.2 %collective-permute-start.29 = (bf16[32,2048]{1,0:T(8,128)(2,1)S(1)}, bf16[32,2048]{1,0:T(8,128)(2,1)S(1)}, u32[]{:S(2)}, u32[]{:S(2)}) collective-permute-start(bf16[32,2048]{1,0:T(8,128)(2,1)S(1)} %get-tuple-element.99), channel_id=1, source_target_pairs={{0,6},{2,4},{4,2},{6,0},{8,14},{10,12},{12,10},{14,8},{16,22},{18,... | collective-permute-start | bytes 393224 | tf_op jit(solution)/shard_map/ppermute | solution.py:389
  109.2 16.3 %collective-permute-start.23 = (bf16[64,2048]{1,0:T(8,128)(2,1)S(1)}, bf16[64,2048]{1,0:T(8,128)(2,1)S(1)}, u32[]{:S(2)}, u32[]{:S(2)}) collective-permute-start(bf16[64,2048]{1,0:T(8,128)(2,1)S(1)} %get-tuple-element.92), channel_id=1, source_target_pairs={{0,2},{2,0},{4,6},{6,4},{8,10},{10,8},{12,14},{14,12},{16,18},{18,... | collective-permute-start | bytes 786440 | tf_op jit(solution)/shard_map/ppermute | solution.py:389
  110.6 14.9 %collective-permute-start.24 = (bf16[64,2048]{1,0:T(8,128)(2,1)S(1)}, bf16[64,2048]{1,0:T(8,128)(2,1)S(1)}, u32[]{:S(2)}, u32[]{:S(2)}) collective-permute-start(bf16[64,2048]{1,0:T(8,128)(2,1)S(1)} %get-tuple-element.93), channel_id=1, source_target_pairs={{0,4},{2,6},{4,0},{6,2},{8,12},{10,14},{12,8},{14,10},{16,20},{18,... | collective-permute-start | bytes 786440 | tf_op jit(solution)/shard_map/ppermute | solution.py:389
  111.5 14.0 %collective-permute-start.25 = (bf16[64,2048]{1,0:T(8,128)(2,1)S(1)}, bf16[64,2048]{1,0:T(8,128)(2,1)S(1)}, u32[]{:S(2)}, u32[]{:S(2)}) collective-permute-start(bf16[64,2048]{1,0:T(8,128)(2,1)S(1)} %get-tuple-element.94), channel_id=1, source_target_pairs={{0,6},{2,4},{4,2},{6,0},{8,14},{10,12},{12,10},{14,8},{16,22},{18,... | collective-permute-start | bytes 786440 | tf_op jit(solution)/shard_map/ppermute | solution.py:389
  113.5 9.1 %collective-permute-start.34 = (bf16[32,2048]{1,0:T(8,128)(2,1)S(1)}, bf16[32,2048]{1,0:T(8,128)(2,1)S(1)}, u32[]{:S(2)}, u32[]{:S(2)}) collective-permute-start(bf16[32,2048]{1,0:T(8,128)(2,1)S(1)} %get-tuple-element.105), channel_id=1, source_target_pairs={{0,4},{2,6},{4,0},{6,2},{8,12},{10,14},{12,8},{14,10},{16,20},{18,... | collective-permute-start | bytes 393224 | tf_op jit(solution)/shard_map/ppermute | solution.py:389
  114.2 9.5 %collective-permute-start.35 = (bf16[32,2048]{1,0:T(8,128)(2,1)S(1)}, bf16[32,2048]{1,0:T(8,128)(2,1)S(1)}, u32[]{:S(2)}, u32[]{:S(2)}) collective-permute-start(bf16[32,2048]{1,0:T(8,128)(2,1)S(1)} %get-tuple-element.106), channel_id=1, source_target_pairs={{0,6},{2,4},{4,2},{6,0},{8,14},{10,12},{12,10},{14,8},{16,22},{18,... | collective-permute-start | bytes 393224 | tf_op jit(solution)/shard_map/ppermute | solution.py:389
  124.2 13.5 %collective-permute-start.36 = (bf16[64,2048]{1,0:T(8,128)(2,1)S(1)}, bf16[64,2048]{1,0:T(8,128)(2,1)S(1)}, u32[]{:S(2)}, u32[]{:S(2)}) collective-permute-start(bf16[64,2048]{1,0:T(8,128)(2,1)S(1)} %shard_map.142), channel_id=1, source_target_pairs={{0,16},{2,18},{4,20},{6,22},{8,24},{10,26},{12,28},{14,30},{16,0},... | collective-permute-start | bytes 786440 | tf_op jit(solution)/shard_map/ppermute | solution.py:386
  126.3 11.4 %collective-permute-start.26 = (bf16[64,2048]{1,0:T(8,128)(2,1)S(1)}, bf16[64,2048]{1,0:T(8,128)(2,1)S(1)}, u32[]{:S(2)}, u32[]{:S(2)}) collective-permute-start(bf16[64,2048]{1,0:T(8,128)(2,1)S(1)} %get-tuple-element.96), channel_id=1, source_target_pairs={{0,8},{2,10},{4,12},{6,14},{8,16},{10,18},{12,20},{14,22},{16,24},... | collective-permute-start | bytes 786440 | tf_op jit(solution)/shard_map/ppermute | solution.py:386
  (20 other events, 134.3 us)

commit v2 on v1

--- a/solution.py
+++ b/solution.py
@@ -293,27 +293,6 @@
     return jax.ShapeDtypeStruct(shape, jnp.bfloat16)
 
 
-def fetch_kernel(*refs):
-    count = (len(refs) - 1) // 2
-    copies = [
-        pltpu.make_async_copy(refs[i], refs[count + i], refs[-1].at[i]) for i in range(count)
-    ]
-    for copy in copies:
-        copy.start()
-    for copy in copies:
-        copy.wait()
-
-
-def fetch(arrays):
-    return call(
-        fetch_kernel,
-        tuple(bf16(*array.shape) for array in arrays),
-        [FAR] * len(arrays),
-        flops=1 << 32,
-        scratch=[pltpu.SemaphoreType.DMA((len(arrays),))],
-    )(*arrays)
-
-
 def expert_kernel(parts, gives, *refs):
     sources, weights, refs = refs[:parts], refs[parts : parts + 6], refs[parts + 6 :]
     total = refs[-1]
@@ -374,7 +353,7 @@
     swap = [(i, (i + 1) % tp) for i in range(tp)]
     mine = (gate_up[0], lin_up[0], down_weight[0])
     other = [lax.ppermute(part, "tp", swap) for part in mine]
-    held, swapped = mine, fetch(other)
+    held, swapped = mine, tuple(other)
     me, half_of = lax.axis_index("sp").reshape(1), lax.axis_index("tp").reshape(1)
 
     inner = heads
@@ -427,7 +406,7 @@
 
     size = max(1, outer // 4)
     groups = [range(i, min(i + size, outer)) for i in range(0, outer, size)]
-    across = outer // 2 if outer > 2 and outer % 2 == 0 and size == 1 else None
+    across = None
     at = {d: (to_plane(rows, d) if d else rows,) for d in blocks if d != across}
 
     def send_slots(places, after):
@@ -466,13 +445,17 @@
         ]
 
     half = (len(groups) + 1) // 2
-    first = [slots[r] for r in range(inner) for slots in sent[:half]]
-    early = run_experts(first, inner, held, swapped, after)
-    second = [slots[r] for slots in reversed(sent[half:]) for r in range(inner)]
-    late = run_experts(second, len(second), held, swapped, early[:1])
-    home = send_home([n for places in groups[:half] for n in places], early)
-    for g, places in enumerate(reversed(groups[half:])):
-        home += send_home(places, late[g * inner : (g + 1) * inner])
+    flat = lambda some: [part for slots in some for part in slots]
+    results, last = {}, after
+    for some in [range(half), *([g] for g in range(len(groups) - 1, half - 1, -1))]:
+        sources = flat(sent[g] for g in some)
+        outs = run_experts(sources, len(sources), held, swapped, last)
+        last = outs[:1]
+        for place, g in enumerate(some):
+            results[g] = outs[place * inner : (place + 1) * inner]
+    home = []
+    for g in reversed(range(len(groups))):
+        home += send_home(groups[g], results[g])
     return call(final_kernel, bf16(own_rows, width), [NEAR] * (1 + len(home)), in_vmem=False)(
         mixed, *home
     )

time: 139 us -> 149 us (1.072)
  the two profiles are of different devices: /device:TPU:0 before, /device:TPU:12 now
where the time goes in v2:
time: 149 us; the launch traced here: 148 us
  starting transfers between devices  54.2 us (36%)
  waiting for transfers between devices  51.5 us (35%)
  Pallas kernels  41.9 us (28%)
    pallas_call x18, Pallas kernels, placed(): run(*(spec.place(arg) for spec, arg in zip(specs, args, strict=True)))  41.9 us
    ppermute x30, starting transfers between devices, in_plane(): return lax.ppermute(part, 'sp', [(i, i ^ near) for i in range(sp)])  36.6 us
    ppermute x30, waiting for transfers between devices, in_plane(): return lax.ppermute(part, 'sp', [(i, i ^ near) for i in range(sp)])  27.2 us
    ppermute x9, waiting for transfers between devices, to_plane(): lax.ppermute(part, 'sp', [(i, (i + distance * inner) % sp) for i in range...  22.7 us
    ppermute x9, starting transfers between devices, to_plane(): lax.ppermute(part, 'sp', [(i, (i + distance * inner) % sp) for i in range...  17.1 us
  transfers between devices with their start and end apart: 43, of which 18 were waited for; matrix products, arithmetic and copies ran while one was open for 0% of the time, Pallas kernels for 28%

profile of v2, /device:TPU:12, one launch (start us, length us, event | category | flops | bytes accessed | tf_op | source)
XLA Modules:
  0.0 147.8 jit_solution(3498657335473367886)
XLA Ops:
  3.9 2.5 %collective-permute-done.refs_1_ = bf16[128,256]{1,0:T(8,128)(2,1)S(1)} collective-permute-done((bf16[128,256]{1,0:T(8,128)(2,1)S(1)}, bf16[128,256]{1,0:T(8,128)(2,1)S(1)}, u32[]{:S(2)}, u32[]{:S(2)}) %collective-permute-start) | collective-permute-done | bytes 65568 | tf_op jit(solution)/shard_map/ppermute | solution.py:368
  7.8 3.7 %collective-permute-done.2.refs_3_ = bf16[128,256]{1,0:T(8,128)(2,1)S(1)} collective-permute-done((bf16[128,256]{1,0:T(8,128)(2,1)S(1)}, bf16[128,256]{1,0:T(8,128)(2,1)S(1)}, u32[]{:S(2)}, u32[]{:S(2)}) %collective-permute-start.2) | collective-permute-done | bytes 65568 | tf_op jit(solution)/shard_map/ppermute | solution.py:368
  14.4 2.3 %collective-permute-done.3.refs_5_ = bf16[136,256]{1,0:T(8,128)(2,1)S(1)} collective-permute-done((bf16[136,256]{1,0:T(8,128)(2,1)S(1)}, bf16[136,256]{1,0:T(8,128)(2,1)S(1)}, u32[]{:S(2)}, u32[]{:S(2)}) %collective-permute-start.3) | collective-permute-done | bytes 69664 | tf_op jit(solution)/shard_map/ppermute | solution.py:365
  16.7 4.8 %collective-permute-start.5 = (bf16[136,256]{1,0:T(8,128)(2,1)S(1)}, bf16[136,256]{1,0:T(8,128)(2,1)S(1)}, u32[]{:S(2)}, u32[]{:S(2)}) collective-permute-start(bf16[136,256]{1,0:T(8,128)(2,1)S(1)} %shard_map.129.refs_4_), channel_id=1, source_target_pairs={{0,16},{2,18},{4,20},{6,22},{8,24},{10,26},{12,28},{14,30},{16,0},... | collective-permute-start | bytes 208904 | tf_op jit(solution)/shard_map/ppermute | solution.py:365
  21.5 2.3 %collective-permute-done.5.refs_7_ = bf16[136,256]{1,0:T(8,128)(2,1)S(1)} collective-permute-done((bf16[136,256]{1,0:T(8,128)(2,1)S(1)}, bf16[136,256]{1,0:T(8,128)(2,1)S(1)}, u32[]{:S(2)}, u32[]{:S(2)}) %collective-permute-start.5) | collective-permute-done | bytes 69664 | tf_op jit(solution)/shard_map/ppermute | solution.py:365
  26.8 2.3 %collective-permute-done.6.refs_1_ = bf16[128,256]{1,0:T(8,128)(2,1)S(1)} collective-permute-done((bf16[128,256]{1,0:T(8,128)(2,1)S(1)}, bf16[128,256]{1,0:T(8,128)(2,1)S(1)}, u32[]{:S(2)}, u32[]{:S(2)}) %collective-permute-start.6) | collective-permute-done | bytes 65568 | tf_op jit(solution)/shard_map/ppermute | solution.py:368
  30.6 3.8 %shard_map.127 = (f32[128,1024]{1,0:T(8,128)S(1)}, f32[128,1024]{1,0:T(8,128)S(1)}, bf16[1024,2048]{1,0:T(8,128)(2,1)S(1)}, bf16[64,2048]{1,0:T(8,128)(2,1)S(1)}, f32[1,2048]{1,0:T(1,128)S(1)}) custom-call(f32[4]{0:T(128)} %decay_ref.9, bf16[128,512]{1,0:T(8,128)(2,1)} %q_ref.3, bf16[128,512]{1,0:T(8,128)(2,1)} %keys_ref.1, bf16[128,1024]{1,0:T(8,128)(2,1)} %values_ref.1, ...), custom_call_target="tpu_custom_call" | custom-call | flops 4294967296 | bytes 1048576 | tf_op jit(solution)/shard_map/pallas_call | solution.py:287
  34.4 2.1 %shard_map.131 = (bf16[64,2048]{1,0:T(8,128)(2,1)S(1)}, bf16[64,2048]{1,0:T(8,128)(2,1)S(1)}) custom-call(s32[1]{0:T(128)} %bitcast.1.me_ref, f32[4]{0:T(128)} %decay_ref.9, s32[1]{0:T(128)} %bitcast.2._.tp_ref, bf16[128,512]{1,0:T(8,128)(2,1)} %q_ref.3, f32[128,1024]{1,0:T(8,128)S(1)} %get-tuple-element.56.intra_ref, ...), custom_call_target="tpu_custom_call" | custom-call | flops 268435456 | bytes 1048576 | tf_op jit(solution)/shard_map/pallas_call | solution.py:287
  40.9 3.5 %collective-permute-done.19.refs_1_ = bf16[32,2048]{1,0:T(8,128)(2,1)S(1)} collective-permute-done((bf16[32,2048]{1,0:T(8,128)(2,1)S(1)}, bf16[32,2048]{1,0:T(8,128)(2,1)S(1)}, u32[]{:S(2)}, u32[]{:S(2)}) %collective-permute-start.19) | collective-permute-done | bytes 131104 | tf_op jit(solution)/shard_map/ppermute | solution.py:368
  45.4 1.6 %collective-permute-start.21 = (bf16[32,2048]{1,0:T(8,128)(2,1)S(1)}, bf16[32,2048]{1,0:T(8,128)(2,1)S(1)}, u32[]{:S(2)}, u32[]{:S(2)}) collective-permute-start(bf16[32,2048]{1,0:T(8,128)(2,1)S(1)} %get-tuple-element.82), channel_id=1, source_target_pairs={{0,6},{2,4},{4,2},{6,0},{8,14},{10,12},{12,10},{14,8},{16,22},{18,... | collective-permute-start | bytes 393224 | tf_op jit(solution)/shard_map/ppermute | solution.py:368
  47.0 4.3 %collective-permute-done.21.refs_3_ = bf16[32,2048]{1,0:T(8,128)(2,1)S(1)} collective-permute-done((bf16[32,2048]{1,0:T(8,128)(2,1)S(1)}, bf16[32,2048]{1,0:T(8,128)(2,1)S(1)}, u32[]{:S(2)}, u32[]{:S(2)}) %collective-permute-start.21) | collective-permute-done | bytes 131104 | tf_op jit(solution)/shard_map/ppermute | solution.py:368
  51.3 2.9 %collective-permute-start.10 = (bf16[64,2048]{1,0:T(8,128)(2,1)S(1)}, bf16[64,2048]{1,0:T(8,128)(2,1)S(1)}, u32[]{:S(2)}, u32[]{:S(2)}) collective-permute-start(bf16[64,2048]{1,0:T(8,128)(2,1)S(1)} %get-tuple-element.72.refs_0_), channel_id=1, source_target_pairs={{0,16},{2,18},{4,20},{6,22},{8,24},{10,26},{12,28},{14,30},{16,0},... | collective-permute-start | bytes 786440 | tf_op jit(solution)/shard_map/ppermute | solution.py:365
  54.2 1.8 %collective-permute-start.11 = (bf16[64,2048]{1,0:T(8,128)(2,1)S(1)}, bf16[64,2048]{1,0:T(8,128)(2,1)S(1)}, u32[]{:S(2)}, u32[]{:S(2)}) collective-permute-start(bf16[64,2048]{1,0:T(8,128)(2,1)S(1)} %get-tuple-element.72.refs_0_), channel_id=1, source_target_pairs={{0,8},{2,10},{4,12},{6,14},{8,16},{10,18},{12,20},{14,22},{16,24},... | collective-permute-start | bytes 786440 | tf_op jit(solution)/shard_map/ppermute | solution.py:365
  56.5 8.1 %collective-permute-done.10.refs_0_ = bf16[64,2048]{1,0:T(8,128)(2,1)S(1)} collective-permute-done((bf16[64,2048]{1,0:T(8,128)(2,1)S(1)}, bf16[64,2048]{1,0:T(8,128)(2,1)S(1)}, u32[]{:S(2)}, u32[]{:S(2)}) %collective-permute-start.10) | collective-permute-done | bytes 262176 | tf_op jit(solution)/shard_map/ppermute | solution.py:365
  65.9 4.1 %collective-permute-done.11.refs_0_ = bf16[64,2048]{1,0:T(8,128)(2,1)S(1)} collective-permute-done((bf16[64,2048]{1,0:T(8,128)(2,1)S(1)}, bf16[64,2048]{1,0:T(8,128)(2,1)S(1)}, u32[]{:S(2)}, u32[]{:S(2)}) %collective-permute-start.11) | collective-permute-done | bytes 262176 | tf_op jit(solution)/shard_map/ppermute | solution.py:365
  73.7 4.6 %collective-permute-done.23.refs_6_ = bf16[32,2048]{1,0:T(8,128)(2,1)S(1)} collective-permute-done((bf16[32,2048]{1,0:T(8,128)(2,1)S(1)}, bf16[32,2048]{1,0:T(8,128)(2,1)S(1)}, u32[]{:S(2)}, u32[]{:S(2)}) %collective-permute-start.23) | collective-permute-done | bytes 131104 | tf_op jit(solution)/shard_map/ppermute | solution.py:368
  83.9 11.5 %shard_map.137 = (bf16[32,2048]{1,0:T(8,128)(2,1)S(1)}, bf16[32,2048]{1,0:T(8,128)(2,1)S(1)}, bf16[32,2048]{1,0:T(8,128)(2,1)S(1)}, bf16[32,2048]{1,0:T(8,128)(2...) custom-call(bf16[32,2048]{1,0:T(8,128)(2,1)S(1)} %get-tuple-element., ...), custom_call_target="tpu_custom_call" | custom-call | flops 6442450944 | bytes 1048576 | tf_op jit(solution)/shard_map/pallas_call | solution.py:287
  96.9 8.3 %shard_map.138 = (bf16[32,2048]{1,0:T(8,128)(2,1)S(1)}, bf16[32,2048]{1,0:T(8,128)(2,1)S(1)}, bf16[32,2048]{1,0:T(8,128)(2,1)S(1)}, bf16[32,2048]{1,0:T(8,128)(2,1)S(1)}) custom-call(bf16[32,2048]{1,0:T(8,128)(2,1)S(1)} %get-tuple-element.76.refs_14_.refs_0_, bf16[32,2048]{1,0:T(8,128)(2,1)S(1)} %collective-permute-done.13.refs_1_, ...), custom_call_target="tpu_custom_call" | custom-call | flops 3221225472 | bytes 1048576 | tf_op jit(solution)/shard_map/pallas_call | solution.py:287
  108.7 8.5 %shard_map.140 = (bf16[32,2048]{1,0:T(8,128)(2,1)S(1)}, bf16[32,2048]{1,0:T(8,128)(2,1)S(1)}, bf16[32,2048]{1,0:T(8,128)(2,1)S(1)}, bf16[32,2048]{1,0:T(8,128)(2,1)S(1)}) custom-call(bf16[32,2048]{1,0:T(8,128)(2,1)S(1)} %get-tuple-element.75.refs_1_.refs_0_, bf16[32,2048]{1,0:T(8,128)(2,1)S(1)} %collective-permute-done.29.refs_1_, ...), custom_call_target="tpu_custom_call" | custom-call | flops 3221225472 | bytes 1048576 | tf_op jit(solution)/shard_map/pallas_call | solution.py:287
  128.7 3.1 %collective-permute-start.35 = (bf16[64,2048]{1,0:T(8,128)(2,1)S(1)}, bf16[64,2048]{1,0:T(8,128)(2,1)S(1)}, u32[]{:S(2)}, u32[]{:S(2)}) collective-permute-start(bf16[64,2048]{1,0:T(8,128)(2,1)S(1)} %shard_map.141), channel_id=1, source_target_pairs={{0,24},{2,26},{4,28},{6,30},{8,0},{10,2},{12,4},{14,6},{16,8},{18,... | collective-permute-start | bytes 786440 | tf_op jit(solution)/shard_map/ppermute | solution.py:365
  134.6 1.6 %collective-permute-start.42 = (bf16[32,2048]{1,0:T(8,128)(2,1)S(1)}, bf16[32,2048]{1,0:T(8,128)(2,1)S(1)}, u32[]{:S(2)}, u32[]{:S(2)}) collective-permute-start(bf16[32,2048]{1,0:T(8,128)(2,1)S(1)} %get-tuple-element.104), channel_id=1, source_target_pairs={{0,6},{2,4},{4,2},{6,0},{8,14},{10,12},{12,10},{14,8},{16,22},{18,... | collective-permute-start | bytes 393224 | tf_op jit(solution)/shard_map/ppermute | solution.py:368
  136.3 2.5 %collective-permute-done.41.refs_2_ = bf16[32,2048]{1,0:T(8,128)(2,1)S(1)} collective-permute-done((bf16[32,2048]{1,0:T(8,128)(2,1)S(1)}, bf16[32,2048]{1,0:T(8,128)(2,1)S(1)}, u32[]{:S(2)}, u32[]{:S(2)}) %collective-permute-start.41) | collective-permute-done | bytes 131104 | tf_op jit(solution)/shard_map/ppermute | solution.py:368
  138.8 1.7 %collective-permute-done.42.refs_3_ = bf16[32,2048]{1,0:T(8,128)(2,1)S(1)} collective-permute-done((bf16[32,2048]{1,0:T(8,128)(2,1)S(1)}, bf16[32,2048]{1,0:T(8,128)(2,1)S(1)}, u32[]{:S(2)}, u32[]{:S(2)}) %collective-permute-start.42) | collective-permute-done | bytes 131104 | tf_op jit(solution)/shard_map/ppermute | solution.py:368
  141.0 5.9 %collective-permute-done.35.refs_1_ = bf16[64,2048]{1,0:T(8,128)(2,1)S(1)} collective-permute-done((bf16[64,2048]{1,0:T(8,128)(2,1)S(1)}, bf16[64,2048]{1,0:T(8,128)(2,1)S(1)}, u32[]{:S(2)}, u32[]{:S(2)}) %collective-permute-start.35) | collective-permute-done | bytes 262176 | tf_op jit(solution)/shard_map/ppermute | solution.py:365
  (86 shorter events, 49.8 us)
Async XLA Ops:
  0.0 80.3 %collective-permute-start.16 = (bf16[2048,1024]{1,0:T(8,128)(2,1)}, bf16[2048,1024]{1,0:T(8,128)(2,1)}, u32[]{:S(2)}, u32[]{:S(2)}) collective-permute-start(bf16[2048,1024]{1,0:T(8,128)(2,1)} %bitcast.8), channel_id=1, source_target_pairs={{0,1},{1,0},{2,3},{3,2},{4,5},{5,4},{6,7},{7,6},{8,9},{9,8},{10,11... | collective-permute-start | bytes 12582920 | tf_op jit(solution)/shard_map/ppermute | solution.py:355
  0.0 81.8 %collective-permute-start.17 = (bf16[2048,1024]{1,0:T(8,128)(2,1)}, bf16[2048,1024]{1,0:T(8,128)(2,1)}, u32[]{:S(2)}, u32[]{:S(2)}) collective-permute-start(bf16[2048,1024]{1,0:T(8,128)(2,1)} %bitcast.12), channel_id=1, source_target_pairs={{0,1},{1,0},{2,3},{3,2},{4,5},{5,4},{6,7},{7,6},{8,9},{9,8},{10,11... | collective-permute-start | bytes 12582920 | tf_op jit(solution)/shard_map/ppermute | solution.py:355
  0.5 82.7 %collective-permute-start.18 = (bf16[1024,2048]{1,0:T(8,128)(2,1)}, bf16[1024,2048]{1,0:T(8,128)(2,1)}, u32[]{:S(2)}, u32[]{:S(2)}) collective-permute-start(bf16[1024,2048]{1,0:T(8,128)(2,1)} %bitcast.16), channel_id=1, source_target_pairs={{0,1},{1,0},{2,3},{3,2},{4,5},{5,4},{6,7},{7,6},{8,9},{9,8},{10,11... | collective-permute-start | bytes 12582920 | tf_op jit(solution)/shard_map/ppermute | solution.py:355
  12.9 8.7 %collective-permute-start.4 = (bf16[136,256]{1,0:T(8,128)(2,1)S(1)}, bf16[136,256]{1,0:T(8,128)(2,1)S(1)}, u32[]{:S(2)}, u32[]{:S(2)}) collective-permute-start(bf16[136,256]{1,0:T(8,128)(2,1)S(1)} %shard_map.129.refs_4_), channel_id=1, source_target_pairs={{0,8},{2,10},{4,12},{6,14},{8,16},{10,18},{12,20},{14,22},{16,24},... | collective-permute-start | bytes 208904 | tf_op jit(solution)/shard_map/ppermute | solution.py:365
  44.3 9.9 %collective-permute-start.12 = (bf16[64,2048]{1,0:T(8,128)(2,1)S(1)}, bf16[64,2048]{1,0:T(8,128)(2,1)S(1)}, u32[]{:S(2)}, u32[]{:S(2)}) collective-permute-start(bf16[64,2048]{1,0:T(8,128)(2,1)S(1)} %get-tuple-element.72.refs_0_), channel_id=1, source_target_pairs={{0,24},{2,26},{4,28},{6,30},{8,0},{10,2},{12,4},{14,6},{16,8},{18,... | collective-permute-start | bytes 786440 | tf_op jit(solution)/shard_map/ppermute | solution.py:365
  51.3 13.2 %collective-permute-start.10 = (bf16[64,2048]{1,0:T(8,128)(2,1)S(1)}, bf16[64,2048]{1,0:T(8,128)(2,1)S(1)}, u32[]{:S(2)}, u32[]{:S(2)}) collective-permute-start(bf16[64,2048]{1,0:T(8,128)(2,1)S(1)} %get-tuple-element.72.refs_0_), channel_id=1, source_target_pairs={{0,16},{2,18},{4,20},{6,22},{8,24},{10,26},{12,28},{14,30},{16,0},... | collective-permute-start | bytes 786440 | tf_op jit(solution)/shard_map/ppermute | solution.py:365
  54.2 15.8 %collective-permute-start.11 = (bf16[64,2048]{1,0:T(8,128)(2,1)S(1)}, bf16[64,2048]{1,0:T(8,128)(2,1)S(1)}, u32[]{:S(2)}, u32[]{:S(2)}) collective-permute-start(bf16[64,2048]{1,0:T(8,128)(2,1)S(1)} %get-tuple-element.72.refs_0_), channel_id=1, source_target_pairs={{0,8},{2,10},{4,12},{6,14},{8,16},{10,18},{12,20},{14,22},{16,24},... | collective-permute-start | bytes 786440 | tf_op jit(solution)/shard_map/ppermute | solution.py:365
  70.1 8.2 %collective-permute-start.23 = (bf16[32,2048]{1,0:T(8,128)(2,1)S(1)}, bf16[32,2048]{1,0:T(8,128)(2,1)S(1)}, u32[]{:S(2)}, u32[]{:S(2)}) collective-permute-start(bf16[32,2048]{1,0:T(8,128)(2,1)S(1)} %get-tuple-element.84), channel_id=1, source_target_pairs={{0,4},{2,6},{4,0},{6,2},{8,12},{10,14},{12,8},{14,10},{16,20},{18,... | collective-permute-start | bytes 393224 | tf_op jit(solution)/shard_map/ppermute | solution.py:368
  71.6 8.1 %collective-permute-start.24 = (bf16[32,2048]{1,0:T(8,128)(2,1)S(1)}, bf16[32,2048]{1,0:T(8,128)(2,1)S(1)}, u32[]{:S(2)}, u32[]{:S(2)}) collective-permute-start(bf16[32,2048]{1,0:T(8,128)(2,1)S(1)} %get-tuple-element.85), channel_id=1, source_target_pairs={{0,6},{2,4},{4,2},{6,0},{8,14},{10,12},{12,10},{14,8},{16,22},{18,... | collective-permute-start | bytes 393224 | tf_op jit(solution)/shard_map/ppermute | solution.py:368
  78.3 17.0 %collective-permute-start.13 = (bf16[32,2048]{1,0:T(8,128)(2,1)S(1)}, bf16[32,2048]{1,0:T(8,128)(2,1)S(1)}, u32[]{:S(2)}, u32[]{:S(2)}) collective-permute-start(bf16[32,2048]{1,0:T(8,128)(2,1)S(1)} %get-tuple-element.77), channel_id=1, source_target_pairs={{0,2},{2,0},{4,6},{6,4},{8,10},{10,8},{12,14},{14,12},{16,18},{18,... | collective-permute-start | bytes 393224 | tf_op jit(solution)/shard_map/ppermute | solution.py:368
  79.7 17.2 %collective-permute-start.14 = (bf16[32,2048]{1,0:T(8,128)(2,1)S(1)}, bf16[32,2048]{1,0:T(8,128)(2,1)S(1)}, u32[]{:S(2)}, u32[]{:S(2)}) collective-permute-start(bf16[32,2048]{1,0:T(8,128)(2,1)S(1)} %get-tuple-element.78), channel_id=1, source_target_pairs={{0,4},{2,6},{4,0},{6,2},{8,12},{10,14},{12,8},{14,10},{16,20},{18,... | collective-permute-start | bytes 393224 | tf_op jit(solution)/shard_map/ppermute | solution.py:368
  80.3 16.5 %collective-permute-start.15 = (bf16[32,2048]{1,0:T(8,128)(2,1)S(1)}, bf16[32,2048]{1,0:T(8,128)(2,1)S(1)}, u32[]{:S(2)}, u32[]{:S(2)}) collective-permute-start(bf16[32,2048]{1,0:T(8,128)(2,1)S(1)} %get-tuple-element.79), channel_id=1, source_target_pairs={{0,6},{2,4},{4,2},{6,0},{8,14},{10,12},{12,10},{14,8},{16,22},{18,... | collective-permute-start | bytes 393224 | tf_op jit(solution)/shard_map/ppermute | solution.py:368
  81.8 25.5 %collective-permute-start.29 = (bf16[32,2048]{1,0:T(8,128)(2,1)S(1)}, bf16[32,2048]{1,0:T(8,128)(2,1)S(1)}, u32[]{:S(2)}, u32[]{:S(2)}) collective-permute-start(bf16[32,2048]{1,0:T(8,128)(2,1)S(1)} %get-tuple-element.91), channel_id=1, source_target_pairs={{0,2},{2,0},{4,6},{6,4},{8,10},{10,8},{12,14},{14,12},{16,18},{18,... | collective-permute-start | bytes 393224 | tf_op jit(solution)/shard_map/ppermute | solution.py:368
  83.2 25.5 %collective-permute-start.30 = (bf16[32,2048]{1,0:T(8,128)(2,1)S(1)}, bf16[32,2048]{1,0:T(8,128)(2,1)S(1)}, u32[]{:S(2)}, u32[]{:S(2)}) collective-permute-start(bf16[32,2048]{1,0:T(8,128)(2,1)S(1)} %get-tuple-element.92), channel_id=1, source_target_pairs={{0,4},{2,6},{4,0},{6,2},{8,12},{10,14},{12,8},{14,10},{16,20},{18,... | collective-permute-start | bytes 393224 | tf_op jit(solution)/shard_map/ppermute | solution.py:368
  95.3 13.4 %collective-permute-start.31 = (bf16[32,2048]{1,0:T(8,128)(2,1)S(1)}, bf16[32,2048]{1,0:T(8,128)(2,1)S(1)}, u32[]{:S(2)}, u32[]{:S(2)}) collective-permute-start(bf16[32,2048]{1,0:T(8,128)(2,1)S(1)} %get-tuple-element.93), channel_id=1, source_target_pairs={{0,6},{2,4},{4,2},{6,0},{8,14},{10,12},{12,10},{14,8},{16,22},{18,... | collective-permute-start | bytes 393224 | tf_op jit(solution)/shard_map/ppermute | solution.py:368
  105.2 14.2 %collective-permute-start.25 = (bf16[32,2048]{1,0:T(8,128)(2,1)S(1)}, bf16[32,2048]{1,0:T(8,128)(2,1)S(1)}, u32[]{:S(2)}, u32[]{:S(2)}) collective-permute-start(bf16[32,2048]{1,0:T(8,128)(2,1)S(1)} %get-tuple-element.88), channel_id=1, source_target_pairs={{0,2},{2,0},{4,6},{6,4},{8,10},{10,8},{12,14},{14,12},{16,18},{18,... | collective-permute-start | bytes 393224 | tf_op jit(solution)/shard_map/ppermute | solution.py:368
  106.6 14.2 %collective-permute-start.26 = (bf16[32,2048]{1,0:T(8,128)(2,1)S(1)}, bf16[32,2048]{1,0:T(8,128)(2,1)S(1)}, u32[]{:S(2)}, u32[]{:S(2)}) collective-permute-start(bf16[32,2048]{1,0:T(8,128)(2,1)S(1)} %get-tuple-element.89), channel_id=1, source_target_pairs={{0,4},{2,6},{4,0},{6,2},{8,12},{10,14},{12,8},{14,10},{16,20},{18,... | collective-permute-start | bytes 393224 | tf_op jit(solution)/shard_map/ppermute | solution.py:368
  107.3 14.9 %collective-permute-start.27 = (bf16[32,2048]{1,0:T(8,128)(2,1)S(1)}, bf16[32,2048]{1,0:T(8,128)(2,1)S(1)}, u32[]{:S(2)}, u32[]{:S(2)}) collective-permute-start(bf16[32,2048]{1,0:T(8,128)(2,1)S(1)} %get-tuple-element.90), channel_id=1, source_target_pairs={{0,6},{2,4},{4,2},{6,0},{8,14},{10,12},{12,10},{14,8},{16,22},{18,... | collective-permute-start | bytes 393224 | tf_op jit(solution)/shard_map/ppermute | solution.py:368
  122.2 9.6 %collective-permute-start.37 = (bf16[32,2048]{1,0:T(8,128)(2,1)S(1)}, bf16[32,2048]{1,0:T(8,128)(2,1)S(1)}, u32[]{:S(2)}, u32[]{:S(2)}) collective-permute-start(bf16[32,2048]{1,0:T(8,128)(2,1)S(1)} %get-tuple-element.100), channel_id=1, source_target_pairs={{0,4},{2,6},{4,0},{6,2},{8,12},{10,14},{12,8},{14,10},{16,20},{18,... | collective-permute-start | bytes 393224 | tf_op jit(solution)/shard_map/ppermute | solution.py:368
  123.7 8.1 %collective-permute-start.38 = (bf16[32,2048]{1,0:T(8,128)(2,1)S(1)}, bf16[32,2048]{1,0:T(8,128)(2,1)S(1)}, u32[]{:S(2)}, u32[]{:S(2)}) collective-permute-start(bf16[32,2048]{1,0:T(8,128)(2,1)S(1)} %get-tuple-element.101), channel_id=1, source_target_pairs={{0,6},{2,4},{4,2},{6,0},{8,14},{10,12},{12,10},{14,8},{16,22},{18,... | collective-permute-start | bytes 393224 | tf_op jit(solution)/shard_map/ppermute | solution.py:368
  125.7 9.0 %collective-permute-start.40 = (bf16[32,2048]{1,0:T(8,128)(2,1)S(1)}, bf16[32,2048]{1,0:T(8,128)(2,1)S(1)}, u32[]{:S(2)}, u32[]{:S(2)}) collective-permute-start(bf16[32,2048]{1,0:T(8,128)(2,1)S(1)} %get-tuple-element.102), channel_id=1, source_target_pairs={{0,2},{2,0},{4,6},{6,4},{8,10},{10,8},{12,14},{14,12},{16,18},{18,... | collective-permute-start | bytes 393224 | tf_op jit(solution)/shard_map/ppermute | solution.py:368
  127.4 13.6 %collective-permute-start.28 = (bf16[64,2048]{1,0:T(8,128)(2,1)S(1)}, bf16[64,2048]{1,0:T(8,128)(2,1)S(1)}, u32[]{:S(2)}, u32[]{:S(2)}) collective-permute-start(bf16[64,2048]{1,0:T(8,128)(2,1)S(1)} %shard_map.139), channel_id=1, source_target_pairs={{0,16},{2,18},{4,20},{6,22},{8,24},{10,26},{12,28},{14,30},{16,0},... | collective-permute-start | bytes 786440 | tf_op jit(solution)/shard_map/ppermute | solution.py:365
  128.7 18.3 %collective-permute-start.35 = (bf16[64,2048]{1,0:T(8,128)(2,1)S(1)}, bf16[64,2048]{1,0:T(8,128)(2,1)S(1)}, u32[]{:S(2)}, u32[]{:S(2)}) collective-permute-start(bf16[64,2048]{1,0:T(8,128)(2,1)S(1)} %shard_map.141), channel_id=1, source_target_pairs={{0,24},{2,26},{4,28},{6,30},{8,0},{10,2},{12,4},{14,6},{16,8},{18,... | collective-permute-start | bytes 786440 | tf_op jit(solution)/shard_map/ppermute | solution.py:365
  132.3 14.7 %collective-permute-start.39 = (bf16[64,2048]{1,0:T(8,128)(2,1)S(1)}, bf16[64,2048]{1,0:T(8,128)(2,1)S(1)}, u32[]{:S(2)}, u32[]{:S(2)}) collective-permute-start(bf16[64,2048]{1,0:T(8,128)(2,1)S(1)} %shard_map.142), channel_id=1, source_target_pairs={{0,8},{2,10},{4,12},{6,14},{8,16},{10,18},{12,20},{14,22},{16,24},... | collective-permute-start | bytes 786440 | tf_op jit(solution)/shard_map/ppermute | solution.py:365
  (22 other events, 260.9 us)
